TPU v7x, 512 devices: a whole 4x8x8 slice. The times are simulated.
512 devices in a mesh: sp: 64 (over z, y), tp: 8 (over x, core).
Axes of the slice: x: 4, y: 8, z: 8, core: 2. Of those that a mesh axis runs over, the one named last changes fastest.
Arguments:
- layer_source_rows: bfloat16 [24576, 2048], P(('sp', 'tp')), may hold values from -6 to 6
- entry_rescale_factor: bfloat16 [2048], replicated, may hold values from 0.099609375 to 1.8984375
- sliding_mixer_entry_matrix: bfloat16 [3, 2048, 1024], P(None, 'sp', 'tp'), may hold values from -0.125 to 0.125
- recurrent_mixer_entry_matrix: bfloat16 [2, 2048, 1024], P(None, 'sp', 'tp'), may hold values from -0.125 to 0.125
- latent_write_read_matrix: bfloat16 [2, 2048, 2048], P(None, 'sp', 'tp'), may hold values from -0.125 to 0.125
- timestep_matrix: bfloat16 [2048, 2, 16], P(None, None, 'tp'), may hold values from -0.125 to 0.125
- sliding_kernel_coefficients: bfloat16 [3, 1024], P(None, 'tp'), may hold values from -3.5 to 3.5
- recurrent_kernel_coefficients: bfloat16 [5, 1024], P(None, 'tp'), may hold values from -0.5 to 0.5
- latent_kernel_coefficients: bfloat16 [5, 2, 2048], P(None, None, 'tp'), may hold values from -0.5 to 0.5
- lane_forgetting_rate: float32 [2, 16], P(None, 'tp'), may hold values from 0 to 1
- spike_forgetting_rate: float32 [24576, 16], P('sp', 'tp'), may hold values from -2 to 0
- lane_rescale_factor: bfloat16 [1024], P('tp'), may hold values from 0.099609375 to 1.8984375
- sliding_mixer_exit_matrix: bfloat16 [1024, 2048], P('tp', 'sp'), may hold values from -0.125 to 0.125
- recurrent_mixer_exit_matrix: bfloat16 [1024, 2048], P('tp', 'sp'), may hold values from -0.125 to 0.125
Outputs:
- mixed_out: bfloat16 [24576, 2048], P(('sp', 'tp'))
All inputs are finite; a program needn't handle non-finite values.
Results may differ from a plain program's by a relative error of at most 0.017.
Values may be sent and summed in bfloat16 or wider, within the bound.
A program may use at most 64 MiB of HBM per device.

v0:
```python
import jax
import jax.numpy as jnp
from jax import lax
from jax.sharding import Mesh
from jax.sharding import PartitionSpec as P

HEAD_DIM = 64
STATE = 128
BLOCK = 128
SP = ("sp_0", "sp_1")
SP_TP = ("sp_0", "sp_1", "tp")


epsilon = 1e-05


def nothing_yet(value, identity):
    return jax.tree.map(
        lambda a, e: jnp.broadcast_to(jnp.asarray(e, a.dtype), a.shape), value, identity
    )


def collected_together(value, axis):
    leaves = jax.tree.leaves(value)
    turns = sorted(range(len(leaves)), key=lambda k: -leaves[k].size)
    width = (1, *leaves[turns[0]].shape)[-1]
    lines = [
        jnp.pad(leaves[k].reshape(-1), (0, -leaves[k].size % width)).reshape(-1, width)
        for k in turns
    ]
    both, at, found = (lax.all_gather(jnp.concatenate(lines), axis), 0, {})
    for k, line in zip(turns, lines):
        share = both[:, at : at + len(line)].reshape(len(both), -1)
        found[k] = share[:, : leaves[k].size].reshape(-1, *leaves[k].shape)
        at += len(line)
    numbers = iter(range(len(leaves)))
    return jax.tree.map(lambda _: found[next(numbers)], value)


def prefix_by_axis(value, axes, combine, identity):
    before = start = nothing_yet(value, identity)
    subtotal = value
    for axis in reversed(axes):
        length, here = (lax.axis_size(axis), lax.axis_index(axis))
        pieces = collected_together(subtotal, axis)
        inside, subtotal = (start, start)
        for k in reversed(range(length)):
            passed = k > here
            subtotal = combine(subtotal, jax.tree.map(lambda part: part[k], pieces))
            inside = jax.tree.map(lambda new, old: jnp.where(passed, new, old), subtotal, inside)
        before = combine(inside, before)
    return before


def carried_in(value, axes, combine, identity):
    before = start = nothing_yet(value, identity)
    subtotal = value
    for axis in reversed(axes):
        length, here = (lax.axis_size(axis), lax.axis_index(axis))
        pieces = jax.tree.map(
            lambda part, kind: lax.all_gather(part.astype(kind), axis),
            subtotal,
            (jnp.bfloat16, jnp.bfloat16),
        )
        inside, subtotal = (start, start)
        for k in range(length):
            passed = k < here
            subtotal = combine(
                subtotal, jax.tree.map(lambda part, own: part[k].astype(own.dtype), pieces, value)
            )
            inside = jax.tree.map(lambda new, old: jnp.where(passed, new, old), subtotal, inside)
        before = combine(inside, before)
    return before


def gather_turned(arrays, axis, dims):
    turned = [jnp.moveaxis(a, dim, 0) for a, dim in zip(arrays, dims)]
    widths = [t[0].size for t in turned]
    both = jnp.concatenate([t.reshape(-1, w) for t, w in zip(turned, widths)], axis=1)
    out = lax.all_gather(both, axis, axis=0, tiled=True)
    pieces = jnp.split(out, [sum(widths[:k]) for k in range(1, len(widths))], axis=1)
    return tuple(
        (
            jnp.moveaxis(b.reshape(-1, *t.shape[1:]), 0, dim)
            for b, t, dim in zip(pieces, turned, dims)
        )
    )


def in_order(pieces, dim):
    dims = list(pieces.shape[1:])
    dims[dim] *= pieces.shape[0]
    return jnp.moveaxis(pieces, 0, dim).reshape(dims)


def from_everyone(value, axis):
    length = lax.axis_size(axis)
    return lax.all_to_all(
        jnp.broadcast_to(value[None], (length, *value.shape)), axis, 0, 0, tiled=True
    )


def gather_directly(value, axis, dim):
    return in_order(from_everyone(value, axis), dim)


def padded_2(value, sides, width):
    for axis, dim in sides:
        size, length = (lax.axis_size(axis), value.shape[dim])
        up = [(i, (i + 1) % size) for i in range(size - 1)]
        down = [(j, i) for i, j in up]
        last = lax.slice_in_dim(value, length - width, length, axis=dim)
        leading = lax.slice_in_dim(value, 0, width, axis=dim)
        before = lax.ppermute(last, axis, up)
        after = lax.ppermute(leading, axis, down)
        value = jnp.concatenate([before, value, after], axis=dim)
    return value


def cut_along(value, dim, length):
    before, after = (value.shape[:dim], value.shape[dim + 1 :])
    return jnp.moveaxis(value.reshape(*before, length, -1, *after), dim, 0)


def sum_at_owner(value, axis, dim):
    length = lax.axis_size(axis)
    pieces = lax.all_to_all(cut_along(value, dim, length), axis, 0, 0, tiled=True)
    return jnp.sum(pieces.astype(jnp.float32), axis=0)


def apply_taps(padded, tap_table, length):
    summed = jnp.zeros((length, padded.shape[1]), jnp.float32)
    for offset in range(tap_table.shape[0]):
        summed = summed + padded[offset : offset + length].astype(jnp.float32) * tap_table[
            offset
        ].astype(jnp.float32)
    return summed


def local_blocks(ssd_x, keys_b, reads_c, timestep_deltas, forgetting_exponent):
    length, groups, per_group, head_dim = ssd_x.shape
    blocks = length // BLOCK
    x_blocks = ssd_x.reshape(blocks, BLOCK, groups, per_group, head_dim)
    b_blocks = keys_b.reshape(blocks, BLOCK, groups, STATE)
    c_blocks = reads_c.reshape(blocks, BLOCK, groups, STATE)
    d_blocks = timestep_deltas.reshape(blocks, BLOCK, groups, per_group)
    l_blocks = forgetting_exponent.reshape(blocks, BLOCK, groups, per_group)
    lower_mask = (jnp.arange(BLOCK)[:, None] >= jnp.arange(BLOCK)[None, :])[None, :, :, None, None]
    running = jnp.cumsum(l_blocks, axis=1)
    log_gaps = jnp.where(lower_mask, running[:, :, None] - running[:, None, :], 0.0)
    decays = jnp.where(lower_mask, jnp.exp(log_gaps), 0.0)
    scores = jnp.einsum("btgn,bsgn->btsg", c_blocks, b_blocks, preferred_element_type=jnp.float32)
    weights = (scores[..., None] * decays * d_blocks[:, None]).astype(jnp.bfloat16)
    within = jnp.einsum("btsgr,bsgrp->btgrp", weights, x_blocks, preferred_element_type=jnp.float32)
    to_end = jnp.exp(running[:, -1:] - running) * d_blocks
    weighted = (x_blocks.astype(jnp.float32) * to_end[..., None]).astype(jnp.bfloat16)
    contribution = jnp.einsum(
        "bsgrp,bsgn->bgrpn", weighted, b_blocks, preferred_element_type=jnp.float32
    )
    return (within, contribution, running, c_blocks)


def combine(earlier, following):
    return (earlier[0] * following[0], earlier[1] * following[0][..., None, None] + following[1])


def run_direction(ssd_x, keys_b, reads_c, timestep_deltas, forgetting_exponent, backward):
    within, contribution, running, c_blocks = local_blocks(
        ssd_x, keys_b, reads_c, timestep_deltas, forgetting_exponent
    )
    block_ends = running[:, -1]

    def chain_step(carry_state, inputs):
        part_state, block_end = inputs
        return (carry_state * jnp.exp(block_end)[..., None, None] + part_state, carry_state)

    summed, before = lax.scan(
        chain_step, jnp.zeros_like(contribution[0]), (contribution, block_ends)
    )
    device_decay = jnp.exp(jnp.sum(block_ends, axis=0))
    identity = (jnp.ones_like(device_decay), jnp.zeros_like(summed))
    if backward:
        incoming = prefix_by_axis((device_decay, summed), SP, combine, identity)
    else:
        incoming = carried_in((device_decay, summed), SP, combine, identity)
    starts = jnp.cumsum(block_ends, axis=0) - block_ends
    entering = (before + incoming[1][None] * jnp.exp(starts)[..., None, None]).astype(jnp.bfloat16)
    carried = jnp.einsum(
        "btgn,bgrpn->btgrp", c_blocks, entering, preferred_element_type=jnp.float32
    )
    carried = carried * jnp.exp(running)[..., None]
    return (within + carried).reshape(ssd_x.shape)


def local(
    layer_source_rows,
    entry_rescale_factor,
    sliding_mixer_entry_matrix,
    recurrent_mixer_entry_matrix,
    latent_write_read_matrix,
    timestep_matrix,
    sliding_kernel_coefficients,
    recurrent_kernel_coefficients,
    latent_kernel_coefficients,
    lane_forgetting_rate,
    spike_forgetting_rate,
    lane_rescale_factor,
    sliding_mixer_exit_matrix,
    recurrent_mixer_exit_matrix,
):
    float_rows = layer_source_rows.astype(jnp.float32)
    normed = (
        float_rows
        * lax.rsqrt(jnp.mean(float_rows * float_rows, axis=-1, keepdims=True) + epsilon)
        * entry_rescale_factor.astype(jnp.float32)
    ).astype(jnp.bfloat16)
    (
        sliding_mixer_entry_matrix,
        recurrent_mixer_entry_matrix,
        latent_write_read_matrix,
        sliding_mixer_exit_matrix,
        recurrent_mixer_exit_matrix,
    ) = gather_turned(
        (
            sliding_mixer_entry_matrix,
            recurrent_mixer_entry_matrix,
            latent_write_read_matrix,
            sliding_mixer_exit_matrix,
            recurrent_mixer_exit_matrix,
        ),
        SP,
        (1, 1, 1, 1, 1),
    )
    conv_width = sliding_mixer_entry_matrix.shape[2]
    ssd_width = recurrent_mixer_entry_matrix.shape[2]
    state_width = latent_write_read_matrix.shape[2]
    local_heads = timestep_matrix.shape[2]
    step_weight = timestep_matrix.reshape(timestep_matrix.shape[0], 2 * local_heads)
    row_piece = gather_directly(normed, "tp", 0)
    row_count = row_piece.shape[0]
    conv_cols = jnp.einsum(
        "rd,kdc->rkc", row_piece, sliding_mixer_entry_matrix, preferred_element_type=jnp.float32
    ).reshape(row_count, -1)
    ssd_cols = jnp.einsum(
        "rd,kdc->rkc", row_piece, recurrent_mixer_entry_matrix, preferred_element_type=jnp.float32
    ).reshape(row_count, -1)
    state_cols = jnp.einsum(
        "rd,kdc->rkc", row_piece, latent_write_read_matrix, preferred_element_type=jnp.float32
    ).reshape(row_count, -1)
    step_cols = jnp.dot(row_piece, step_weight, preferred_element_type=jnp.float32)
    projected = jnp.concatenate([conv_cols, ssd_cols, state_cols, step_cols], axis=1).astype(
        jnp.bfloat16
    )
    length = projected.shape[0]
    out_gate = projected[:, :conv_width]
    in_gate = projected[:, conv_width : 2 * conv_width]
    values = projected[:, 2 * conv_width : 3 * conv_width]
    gate_start = 3 * conv_width
    ssd_gate = projected[:, gate_start : gate_start + ssd_width]
    joined = projected[:, gate_start + ssd_width : gate_start + 2 * ssd_width + 2 * state_width]
    raw_step = projected[:, gate_start + 2 * ssd_width + 2 * state_width :].reshape(
        length, 2, local_heads
    )
    gated_in = (in_gate.astype(jnp.float32) * values.astype(jnp.float32)).astype(jnp.bfloat16)
    padded_both = padded_2(jnp.concatenate([gated_in, joined], axis=1), ((SP, 0),), 2)
    gated_pad = padded_both[1:-1, :conv_width]
    joined_pad = padded_both[:, conv_width:]
    y_conv = (
        out_gate.astype(jnp.float32) * apply_taps(gated_pad, sliding_kernel_coefficients, length)
    ).astype(jnp.bfloat16)
    joined_taps = jnp.concatenate(
        [
            recurrent_kernel_coefficients,
            latent_kernel_coefficients.reshape(latent_kernel_coefficients.shape[0], -1),
        ],
        axis=1,
    )
    mixed_ssd = jax.nn.silu(apply_taps(joined_pad, joined_taps, length)).astype(jnp.bfloat16)
    local_groups = state_width // STATE
    per_group = local_heads // local_groups
    ssd_x = mixed_ssd[:, :ssd_width].reshape(length, local_groups, per_group, HEAD_DIM)
    keys_b = mixed_ssd[:, ssd_width : ssd_width + state_width].reshape(length, local_groups, STATE)
    reads_c = mixed_ssd[:, ssd_width + state_width :].reshape(length, local_groups, STATE)
    timestep_deltas = jax.nn.softplus(raw_step.astype(jnp.float32))
    forgetting_exponent = (
        -timestep_deltas * lane_forgetting_rate[None] + spike_forgetting_rate[:, None, :]
    )
    head_shape = (length, local_groups, per_group)
    y_fwd = run_direction(
        ssd_x,
        keys_b,
        reads_c,
        timestep_deltas[:, 0].reshape(head_shape),
        forgetting_exponent[:, 0].reshape(head_shape),
        False,
    )
    y_bwd = jnp.flip(
        run_direction(
            jnp.flip(ssd_x, 0),
            jnp.flip(keys_b, 0),
            jnp.flip(reads_c, 0),
            jnp.flip(timestep_deltas[:, 1].reshape(head_shape), 0),
            jnp.flip(forgetting_exponent[:, 1].reshape(head_shape), 0),
            True,
        ),
        0,
    )
    gated_out = (y_fwd + y_bwd).reshape(length, ssd_width) * jax.nn.silu(
        ssd_gate.astype(jnp.float32)
    )
    grouped = gated_out.reshape(length, local_groups, per_group * HEAD_DIM)
    grouped = grouped * lax.rsqrt(jnp.mean(grouped * grouped, axis=-1, keepdims=True) + epsilon)
    y_ssd = (grouped.reshape(length, ssd_width) * lane_rescale_factor.astype(jnp.float32)).astype(
        jnp.bfloat16
    )
    mixed_out = sum_at_owner(
        (
            jnp.dot(y_conv, sliding_mixer_exit_matrix, preferred_element_type=jnp.float32)
            + jnp.dot(y_ssd, recurrent_mixer_exit_matrix, preferred_element_type=jnp.float32)
        ).astype(jnp.bfloat16),
        "tp",
        0,
    )
    return mixed_out.astype(jnp.bfloat16)


def solution(mesh):
    torus = Mesh(mesh.devices.reshape(8, 8, mesh.shape["tp"]), ("sp_0", "sp_1", "tp"))
    return jax.shard_map(
        local,
        mesh=torus,
        in_specs=(
            P(SP_TP, None),
            P(),
            P(None, SP, "tp"),
            P(None, SP, "tp"),
            P(None, SP, "tp"),
            P(None, None, "tp"),
            P(None, "tp"),
            P(None, "tp"),
            P(None, None, "tp"),
            P(None, "tp"),
            P(SP, "tp"),
            P("tp"),
            P("tp", SP),
            P("tp", SP),
        ),
        out_specs=P(SP_TP, None),
        check_vma=False,
    )
```

profile of v0, /device:TPU:1, one launch (start us, length us, event | category | flops | bytes accessed | tf_op | source)
XLA Modules:
  0.0 292.5 jit_solution(10762341828514421289)
XLA Ops:
  6.5 0.7 copy-done
  7.3 0.8 copy.242
  8.0 0.7 bitcast_dynamic-update-slice_fusion.3
  8.8 0.7 constant_dynamic-update-slice_fusion.1
  9.5 0.7 constant_dynamic-update-slice_fusion
  10.2 0.6 copy-done.10
  10.8 0.7 convert_element_type.526
  11.5 1.1 fusion.33
  12.6 1.1 fusion.35
  13.7 1.4 broadcast_in_dim.40
  15.0 10.5 %all-to-all-start = ((bf16[8,48,2048]{2,1,0:T(8,128)(2,1)}), bf16[8,48,2048]{2,1,0:T(8,128)(2,1)S(1)}, u32[]{:S(2)}, u32[]{:S(2)}) async-start(bf16[8,48,2048]{2,1,0:T(8,128)(2,1)} %broadcast_in_dim.40), calls=%async_computation | async-start | bytes 3145728 | tf_op jit(solution)/shard_map/all_to_all | solution.py:98
  25.7 1.2 dynamic-slice
  27.6 0.6 bitcast_convert_fusion.2
  28.1 18.0 %all-to-all-done = bf16[8,48,2048]{2,1,0:T(8,128)(2,1)S(1)} async-done(((bf16[8,48,2048]{2,1,0:T(8,128)(2,1)}), bf16[8,48,2048]{2,1,0:T(8,128)(2,1)S(1)}, u32[]{:S(2)}, u32[]{:S(2)}) %all-to-all-start) | async-done | bytes 1572896 | tf_op jit(solution)/shard_map/all_to_all | solution.py:98
  46.1 0.5 fusion.27
  48.3 11.3 %all-reduce.2 = bf16[16]{0:T(256)(128)(2,1)S(1)} all-reduce(bf16[16]{0:T(256)(128)(2,1)S(1)} %dynamic-update-slice), channel_id=2, replica_groups=mesh['sp_0'=8,'sp_1'=8,'tp'=8] {'sp_1'}, use_global_device_ids=true, to_apply=%add.2 | all-reduce | flops 16 | bytes 64
  59.8 0.6 convert_element_type.613
  60.4 17.7 %all_gather.35 = bf16[8,2,1]{2,1,0:T(2,128)(2,1)S(1)} all-gather(bf16[1,2,1]{2,1,0:T(2,128)(2,1)S(1)} %copy.194), channel_id=1, replica_groups=mesh['sp_0'=8,'sp_1'=8,'tp'=8] {'sp_0'}, dimensions={0}, use_global_device_ids=true | all-gather | bytes 36 | tf_op jit(solution)/shard_map/all_gather | solution.py:61
  79.0 0.6 slice_bitcast_fusion.10
  80.1 0.7 multiply_reduce_fusion
  80.8 0.6 broadcast_select_fusion.15
  81.4 0.7 slice_convert_fusion.11
  82.1 0.6 bitcast_exponential_fusion.1
  82.7 0.6 bitcast_exponential_fusion
  83.3 19.5 %all-gather.8.cloned.1.call-done = bf16[2048,1408]{1,0:T(8,128)(2,1)} async-done(((bf16[32,1408]{1,0:T(8,128)(2,1)}), bf16[2048,1408]{1,0:T(8,128)(2,1)}) %all-gather.8.cloned.1.call-update) | async-done | bytes 5767184 | tf_op jit(solution)/shard_map/all_gather | solution.py:80
  102.8 1.2 slice-done
  104.0 1.2 reshape.1186
  105.2 2.0 convolution_convert_fusion.1
  107.2 3.1 %split.22 = bf16[2048,512]{1,0:T(8,128)(2,1)} slice(bf16[2048,1408]{1,0:T(8,128)(2,1)} %all-gather.8.cloned.1.call-done), slice={[0:2048], [640:1152]} | slice | bytes 4194304 | tf_op jit(solution)/shard_map/split | solution.py:81
  110.3 2.5 reshape.1187
  112.9 0.5 copy.246
  113.4 0.9 copy-done.2
  114.3 1.3 convolution_convert_fusion
  115.6 2.7 split.20
  118.3 2.7 copy.176
  121.0 2.4 fusion.8
  123.7 3.0 %collective-permute-start = (bf16[2,768]{0,1:T(8,128)(2,1)S(1)}, bf16[2,768]{0,1:T(8,128)(2,1)S(1)}, u32[]{:S(2)}, u32[]{:S(2)}) collective-permute-start(bf16[2,768]{0,1:T(8,128)(2,1)S(1)} %get-tuple-element.220), channel_id=1, source_target_pairs={{0,8},{8,16},{16,24},{24,32},{32,40},{40,48},{48,56},{56,64},{64,7... | collective-permute-start | bytes 9224 | tf_op jit(solution)/shard_map/ppermute | solution.py:114
  126.7 1.3 collective-permute-start.1
  128.1 0.7 copy.211
  128.9 0.7 copy.230
  129.5 3.6 %collective-permute-done.1 = bf16[2,768]{0,1:T(8,128)(2,1)S(1)} collective-permute-done((bf16[2,768]{0,1:T(8,128)(2,1)S(1)}, bf16[2,768]{0,1:T(8,128)(2,1)S(1)}, u32[]{:S(2)}, u32[]{:S(2)}) %collective-permute-start.1) | collective-permute-done | bytes 3104 | tf_op jit(solution)/shard_map/ppermute | solution.py:115
  133.1 0.4 maximum_maximum_fusion
  133.6 1.4 multiply_convert_fusion
  135.1 0.3 rev.22
  136.2 0.4 while.27
  136.5 20.4 %all-gather.4 = f32[8,129,128]{2,1,0:T(8,128)S(1)} all-gather(f32[1,129,128]{2,1,0:T(8,128)S(1)} %maximum_bitcast_fusion), channel_id=4, replica_groups=mesh['sp_0'=8,'sp_1'=8,'tp'=8] {'sp_1'}, dimensions={0}, use_global_device_ids=true | all-gather | bytes 594432 | tf_op jit(solution)/shard_map/all_gather | solution.py:31
  157.0 0.6 broadcast_select_fusion.7
  159.1 21.1 %all-gather.5 = f32[8,129,128]{2,1,0:T(8,128)S(1)} all-gather(f32[1,129,128]{2,1,0:T(8,128)S(1)} %maximum_bitcast_fusion.1), channel_id=5, replica_groups=mesh['sp_0'=8,'sp_1'=8,'tp'=8] {'sp_0'}, dimensions={0}, use_global_device_ids=true | all-gather | bytes 594432 | tf_op jit(solution)/shard_map/all_gather | solution.py:31
  180.2 0.8 fusion.125
  181.0 0.8 fusion.126
  182.4 0.4 while.26
  182.8 18.6 %all-gather.1 = bf16[16,1,64,128]{3,2,1,0:T(8,128)(2,1)S(1)} all-gather(bf16[2,1,64,128]{3,2,1,0:T(8,128)(2,1)S(1)} %convert_element_type.561), channel_id=3, replica_groups=mesh['sp_0'=8,'sp_1'=8,'tp'=8] {'sp_1'}, dimensions={0}, use_global_device_ids=true | all-gather | bytes 294912 | tf_op jit(solution)/shard_map/all_gather | solution.py:61
  201.6 19.2 %all_gather.38 = bf16[8,2,1,64,128]{4,3,2,1,0:T(8,128)(2,1)S(1)} all-gather(bf16[1,2,1,64,128]{4,3,2,1,0:T(8,128)(2,1)S(1)} %fusion.111), channel_id=1, replica_groups=mesh['sp_0'=8,'sp_1'=8,'tp'=8] {'sp_0'}, dimensions={0}, use_global_device_ids=true | all-gather | bytes 294912 | tf_op jit(solution)/shard_map/all_gather | solution.py:61
  221.1 0.6 multiply_bitcast_fusion
  222.2 1.9 fusion.20
  224.2 1.4 select_add_fusion
  225.8 1.2 fusion.23
  227.4 0.4 fusion.18
  228.1 0.3 fusion.102
  228.4 0.3 fusion.26
  228.9 1.9 fusion.31
  230.8 1.6 add_convert_fusion
  232.5 52.2 %all_to_all.10 = bf16[8,48,2048]{2,1,0:T(8,128)(2,1)S(1)} all-to-all(bf16[8,48,2048]{2,1,0:T(8,128)(2,1)S(1)} %bitcast.521), channel_id=1, replica_groups=mesh['sp_0'=8,'sp_1'=8,'tp'=8] {'tp'}, dimensions={0} | all-to-all | bytes 3145728 | tf_op jit(solution)/shard_map/all_to_all | solution.py:127
  284.7 0.9 reduce_sum.52
  (253 shorter events, 8.6 us)
Async XLA Ops:
  6.5 96.2 %all-gather.8.cloned.1.call-start = ((), (), s32[]{:S(2)}) async-start(), calls=%async_computation.2 | async-start | bytes 5857280 | tf_op jit(solution)/shard_map/all_gather | solution.py:80
  15.0 10.6 %copy-start.18 = (bf16[5,2,256]{2,1,0:T(2,128)(2,1)S(1)}, bf16[5,2,256]{2,1,0:T(2,128)(2,1)}, u32[]{:S(2)}) copy-start(bf16[5,2,256]{2,1,0:T(2,128)(2,1)} %param.26) | copy-start | bytes 15364
  15.0 10.6 %copy-start.11 = (bf16[2048,2,2]{0,2,1:T(2,128)(2,1)S(1)}, bf16[2048,2,2]{0,2,1:T(2,128)(2,1)}, u32[]{:S(2)}) copy-start(bf16[2048,2,2]{0,2,1:T(2,128)(2,1)} %param.23) | copy-start | bytes 49156
  15.0 12.4 %copy-start.56 = (bf16[5,128]{1,0:T(8,128)(2,1)S(1)}, bf16[5,128]{1,0:T(8,128)(2,1)}, u32[]{:S(2)}) copy-start(bf16[5,128]{1,0:T(8,128)(2,1)} %param.25) | copy-start | bytes 3844
  15.0 12.5 %copy-start.37 = (bf16[3,128]{1,0:T(4,128)(2,1)S(1)}, bf16[3,128]{1,0:T(4,128)(2,1)}, u32[]{:S(2)}) copy-start(bf16[3,128]{1,0:T(4,128)(2,1)} %param.24) | copy-start | bytes 2308
  15.0 31.1 %all-to-all-start = ((bf16[8,48,2048]{2,1,0:T(8,128)(2,1)}), bf16[8,48,2048]{2,1,0:T(8,128)(2,1)S(1)}, u32[]{:S(2)}, u32[]{:S(2)}) async-start(bf16[8,48,2048]{2,1,0:T(8,128)(2,1)} %broadcast_in_dim.40), calls=%async_computation | async-start | bytes 3145728 | tf_op jit(solution)/shard_map/all_to_all | solution.py:98
  25.5 21.2 %copy-start.36 = (f32[384,2]{0,1:T(2,128)S(1)}, f32[384,2]{0,1:T(2,128)}, u32[]{:S(2)}) copy-start(f32[384,2]{0,1:T(2,128)} %param.28) | copy-start | bytes 9220
  25.5 21.2 %copy-start.66 = (f32[2,2]{1,0:T(2,128)S(1)}, f32[2,2]{1,0:T(2,128)}, u32[]{:S(2)}) copy-start(f32[2,2]{1,0:T(2,128)} %param.27) | copy-start | bytes 52
  46.1 59.1 %copy-start.1 = (bf16[8,48,2048]{2,1,0:T(8,128)(2,1)}, bf16[8,48,2048]{2,1,0:T(8,128)(2,1)S(1)}, u32[]{:S(2)}) copy-start(bf16[8,48,2048]{2,1,0:T(8,128)(2,1)S(1)} %all-to-all-done) | copy-start | bytes 4718596
  46.6 13.2 %copy-start.68 = (bf16[128]{0:T(256)(128)(2,1)S(1)}, bf16[128]{0:T(256)(128)(2,1)}, u32[]{:S(2)}) copy-start(bf16[128]{0:T(256)(128)(2,1)} %param.29) | copy-start | bytes 772
  78.4 26.8 %copy-start.14 = (f32[3,128,2,1]{1,2,0,3:T(2,128)}, f32[3,128,2,1]{1,2,0,3:T(2,128)S(1)}, u32[]{:S(2)}) copy-start(f32[3,128,2,1]{1,2,0,3:T(2,128)S(1)} %copy.219) | copy-start | bytes 9220
  79.9 25.3 %copy-start.15 = (f32[384,2,1]{0,1,2:T(2,128)}, f32[384,2,1]{0,1,2:T(2,128)S(1)}, u32[]{:S(2)}) copy-start(f32[384,2,1]{0,1,2:T(2,128)S(1)} %rev.26) | copy-start | bytes 9220
  112.9 1.4 copy-start.2
  118.3 2.8 copy-start.3
  123.5 10.1 %copy-start.4 = (bf16[384,384]{0,1:T(8,128)(2,1)}, bf16[384,384]{0,1:T(8,128)(2,1)S(1)}, u32[]{:S(2)}) copy-start(bf16[384,384]{0,1:T(8,128)(2,1)S(1)} %fusion.8) | copy-start | bytes 884740
  123.7 5.9 %collective-permute-start = (bf16[2,768]{0,1:T(8,128)(2,1)S(1)}, bf16[2,768]{0,1:T(8,128)(2,1)S(1)}, u32[]{:S(2)}, u32[]{:S(2)}) collective-permute-start(bf16[2,768]{0,1:T(8,128)(2,1)S(1)} %get-tuple-element.220), channel_id=1, source_target_pairs={{0,8},{8,16},{16,24},{24,32},{32,40},{40,48},{48,56},{56,64},{64,7... | collective-permute-start | bytes 9224 | tf_op jit(solution)/shard_map/ppermute | solution.py:114
  126.7 6.4 %collective-permute-start.1 = (bf16[2,768]{0,1:T(8,128)(2,1)S(1)}, bf16[2,768]{0,1:T(8,128)(2,1)S(1)}, u32[]{:S(2)}, u32[]{:S(2)}) collective-permute-start(bf16[2,768]{0,1:T(8,128)(2,1)S(1)} %get-tuple-element.221), channel_id=1, source_target_pairs={{8,0},{16,8},{24,16},{32,24},{40,32},{48,40},{56,48},{64,56},{72,6... | collective-permute-start | bytes 9224 | tf_op jit(solution)/shard_map/ppermute | solution.py:115
  156.9 1.9 copy-start.39
  156.9 1.9 copy-start.40
  156.9 1.9 copy-start.41
  156.9 1.9 copy-start.42
  157.0 1.9 copy-start.43
  157.0 1.9 copy-start.44
  157.0 23.3 %copy-start.38 = (f32[2]{0:T(128)}, f32[2]{0:T(128)S(1)}, u32[]{:S(2)}) copy-start(f32[2]{0:T(128)S(1)} %get-tuple-element.257) | copy-start | bytes 28
  182.1 19.3 %copy-start.19 = (f32[2]{0:T(128)S(1)}, f32[2]{0:T(128)}, u32[]{:S(2)}) copy-start(f32[2]{0:T(128)} %get-tuple-element.273) | copy-start | bytes 28
  182.1 19.3 %copy-start.21 = (f32[2]{0:T(128)S(1)}, f32[2]{0:T(128)}, u32[]{:S(2)}) copy-start(f32[2]{0:T(128)} %get-tuple-element.274) | copy-start | bytes 28
  182.1 19.3 %copy-start.23 = (f32[2]{0:T(128)S(1)}, f32[2]{0:T(128)}, u32[]{:S(2)}) copy-start(f32[2]{0:T(128)} %get-tuple-element.275) | copy-start | bytes 28
  182.1 19.3 %copy-start.25 = (f32[2]{0:T(128)S(1)}, f32[2]{0:T(128)}, u32[]{:S(2)}) copy-start(f32[2]{0:T(128)} %get-tuple-element.276) | copy-start | bytes 28
  182.1 19.3 %copy-start.27 = (f32[2]{0:T(128)S(1)}, f32[2]{0:T(128)}, u32[]{:S(2)}) copy-start(f32[2]{0:T(128)} %get-tuple-element.277) | copy-start | bytes 28
  182.1 19.3 %copy-start.29 = (f32[2]{0:T(128)S(1)}, f32[2]{0:T(128)}, u32[]{:S(2)}) copy-start(f32[2]{0:T(128)} %get-tuple-element.278) | copy-start | bytes 28
  182.1 19.3 %copy-start.31 = (f32[2]{0:T(128)S(1)}, f32[2]{0:T(128)}, u32[]{:S(2)}) copy-start(f32[2]{0:T(128)} %get-tuple-element.279) | copy-start | bytes 28
  182.1 19.3 %copy-start.33 = (f32[2]{0:T(128)S(1)}, f32[2]{0:T(128)}, u32[]{:S(2)}) copy-start(f32[2]{0:T(128)} %get-tuple-element.272) | copy-start | bytes 28
  220.8 3.3 %copy-start.5 = (f32[1,128,128]{2,1,0:T(8,128)S(1)}, f32[1,128,128]{2,1,0:T(8,128)}, u32[]{:S(2)}) copy-start(f32[1,128,128]{2,1,0:T(8,128)} %get-tuple-element.222) | copy-start | bytes 196612
  221.8 2.3 copy-start.6
  221.9 2.3 copy-start.46
  221.9 2.3 copy-start.47
  221.9 2.3 copy-start.48
  221.9 2.3 copy-start.49
  221.9 2.3 copy-start.50
  221.9 2.3 copy-start.51
  221.9 2.3 copy-start.52
  221.9 3.9 %copy-start.13 = (f32[3,128,2]{1,2,0:T(2,128)S(1)}, f32[3,128,2]{1,2,0:T(2,128)}, u32[]{:S(2)}) copy-start(f32[3,128,2]{1,2,0:T(2,128)} %get-tuple-element.266) | copy-start | bytes 9220
  221.9 3.9 %copy-start.17 = (f32[3,2]{1,0:T(4,128)S(1)}, f32[3,2]{1,0:T(4,128)}, u32[]{:S(2)}) copy-start(f32[3,2]{1,0:T(4,128)} %copy.230) | copy-start | bytes 76
  222.2 2.0 copy-start.7
  222.2 2.0 copy-start.8
  222.2 2.0 copy-start.9
  224.1 3.3 %copy-start.35 = (f32[3,128,2]{1,2,0:T(2,128)S(1)}, f32[3,128,2]{1,2,0:T(2,128)}, u32[]{:S(2)}) copy-start(f32[3,128,2]{1,2,0:T(2,128)} %get-tuple-element.246) | copy-start | bytes 9220
  225.7 2.2 copy-start.20
  225.7 2.2 copy-start.22
  225.7 2.2 copy-start.24
  225.7 2.2 copy-start.26
  225.7 2.2 copy-start.28
  225.7 2.2 copy-start.30
  225.7 2.2 copy-start.32
  225.7 2.2 copy-start.34
  225.7 2.2 copy-start.57
  225.7 2.2 copy-start.58
  225.8 2.2 copy-start.59
  225.8 2.2 copy-start.60
  225.8 2.2 copy-start.61
  225.8 2.2 copy-start.62
  225.8 2.2 copy-start.63
  225.8 2.2 copy-start.64
  225.8 2.2 copy-start.65
  (10 other events, 11.0 us)
Sparse Core Ops, SparseCore 0:
  11.0 91.7 all-gather.7
where the time goes:
time: 294 us; the launch traced here: 292 us
  blocking collectives  161 us (55%)
  waiting for transfers between devices  41 us (14%)
  local copies, waits for them, and re-layouts  31.4 us (11%)
  other arithmetic  15.3 us (5%)
  between operations  15.3 us (5%)
  starting transfers between devices  14.7 us (5%)
  matrix products  13.9 us (5%)
    all_gather x3, blocking collectives, carried_in(): lax.all_gather(part.astype(kind), axis)  55.6 us
    all_to_all x1, blocking collectives, sum_at_owner(): lax.all_to_all(cut_along(value, dim, length), axis, 0, 0, tiled=True)  52.2 us
    all_gather x2, blocking collectives, collected_together(): both, at, found = (lax.all_gather(jnp.concatenate(lines), axis), 0, {})  41.5 us
    all_gather x1, waiting for transfers between devices, gather_turned(): out = lax.all_gather(both, axis, axis=0, tiled=True)  19.5 us
    all_to_all x1, waiting for transfers between devices, from_everyone(): lax.all_to_all(jnp.broadcast_to(value[None], (length, *value.shape)), axi...  18 us
    unnamed x1, blocking collectives  11.3 us
    all_to_all x1, starting transfers between devices, from_everyone(): lax.all_to_all(jnp.broadcast_to(value[None], (length, *value.shape)), axi...  10.5 us
    split x5, local copies, waits for them, and re-layouts, gather_turned(): jnp.split(out, [sum(widths[:k]) for k in range(1, len(widths))], axis=1)  9.78 us
  transfers between devices with their start and end apart: 4, of which 3 were waited for; matrix products, arithmetic and copies ran while one was open for 5% of the time, Pallas kernels for 0%

commit v1 on v0

v1 whole, which is shorter than its diff:
```python
import functools

import jax
import jax.numpy as jnp
from jax import lax
from jax.experimental import pallas as pl
from jax.experimental.pallas import tpu as pltpu
from jax.sharding import PartitionSpec as P

HEAD = 64
STATE = 128
CH = 128
EDGE = 16
EPS = 1e-05
BF = jnp.bfloat16
F32 = jnp.float32
MESH_IDS = pl.DeviceIdType.MESH


def wide(v):
    return v.astype(F32)


def dot_nt(a, b):
    return lax.dot_general(a, b, (((1,), (1,)), ((), ())), preferred_element_type=F32)


def dot_tn(a, b):
    return lax.dot_general(a, b, (((0,), (0,)), ((), ())), preferred_element_type=F32)


def silu(v):
    return v * jax.nn.sigmoid(v)


def softplus(v):
    return jnp.maximum(v, 0.0) + jnp.log1p(jnp.exp(-jnp.abs(v)))


def layer(
    n,
    tps,
    x_ref,
    gain_ref,
    slide_ref,
    rec_ref,
    lat_ref,
    step_ref,
    ctap_ref,
    xtap_ref,
    ltap_ref,
    rate_ref,
    spike_ref,
    lane_ref,
    cexit_ref,
    sexit_ref,
    out_ref,
    abuf,
    w1,
    w2,
    p1,
    p2,
    mixed,
    ycat,
    yacc,
    sb1,
    rb1,
    sb2,
    rb2,
    sb3,
    rb3,
    pre,
    prd,
    obf,
    prx,
    xsend,
    xrecv,
    s1,
    r1,
    s2,
    r2,
    ps,
    pr,
    asem,
    arem,
    hs,
    hr,
    es,
    er,
    os_,
    or_,
    xs,
    xr,
):
    rows = x_ref.shape[0]
    dim = x_ref.shape[1]
    nx = tps // 2
    length = rows * tps
    half = n // 2
    sl = HEAD // n
    ncol = os_.shape[0]
    wcol = dim // ncol
    sp = lax.axis_index("sp")
    tp = lax.axis_index("tp")
    z = sp // n
    y = sp % n
    cx = tp // 2
    core = tp % 2

    def remote(src, dst, ss, rs, zz, yy, tt):
        return pltpu.make_async_remote_copy(
            src_ref=src,
            dst_ref=dst,
            send_sem=ss,
            recv_sem=rs,
            device_id=(zz * n + yy, tt),
            device_id_type=MESH_IDS,
        )

    bar = pltpu.get_barrier_semaphore()

    def greet(s, t):
        pl.semaphore_signal(bar, inc=1, device_id=(s, t), device_id_type=MESH_IDS)

    for k in range(1, n):
        greet(z * n + (y + k) % n, tp)
        greet(((z + k) % n) * n + y, tp)
    for k in range(1, tps):
        greet(sp, (tp + k) % tps)
    greet((sp + 1) % (n * n), tp)
    greet((sp + n * n - 1) % (n * n), tp)

    xf = wide(x_ref[...])
    scale = lax.rsqrt(jnp.mean(xf * xf, axis=-1, keepdims=True) + EPS)
    own_rows = pl.ds(pl.multiple_of(EDGE + rows * tp, 16), rows)
    abuf[own_rows, :] = (xf * scale * wide(gain_ref[...])).astype(BF)

    @pl.when(sp == 0)
    def _():
        abuf[pl.ds(0, EDGE), :] = jnp.zeros((EDGE, dim), BF)

    @pl.when(sp == n * n - 1)
    def _():
        abuf[pl.ds(EDGE + length, EDGE), :] = jnp.zeros((EDGE, dim), BF)

    for h in range(2):
        cut = slice(16 * h, 16 * h + 16)
        w1[z, y, h, :, 0:128] = rec_ref[1, cut, :]
        w1[z, y, h, :, 128:384] = lat_ref[0, cut, :]
        w1[z, y, h, :, 384:640] = lat_ref[1, cut, :]
        w2[z, y, h, :, 0:128] = slide_ref[0, cut, :]
        w2[z, y, h, :, 128:256] = slide_ref[1, cut, :]
        w2[z, y, h, :, 256:384] = slide_ref[2, cut, :]
        w2[z, y, h, :, 384:512] = rec_ref[0, cut, :]
        w2[z, y, h, :, 512:640] = cexit_ref[cut, :]
        w2[z, y, h, :, 640:768] = sexit_ref[cut, :]

    pl.semaphore_wait(bar, 2 * (n - 1) + (tps - 1) + 2)

    def moved(h, phase, k):
        on_y = (h == 0) == (phase == 1)
        return (z, (y + k + n) % n) if on_y else ((z + k + n) % n, y)

    def piece(h, c, s, d):
        off = -((c + 1) // 2) if c % 2 else c // 2
        return place(h, off, s, d)

    def place(h, off, s, d):
        if h == 0:
            return (z - d * s + n) % n, (y + off + n) % n, 0
        return (z + off + n) % n, (y - d * s + n) % n, 1

    def ring_one(w, ss, rs, qs, qr, rnd):
        def first(h, c, nxt):
            d = 1 if nxt % 2 else -1
            ref = w.at[piece(h, c, 0, 1)]
            zz, yy = moved(h, 1, d)
            return remote(ref, ref, qs.at[rnd, h, nxt], qr.at[rnd, h, nxt], zz, yy, tp)

        def first_in(h, c):
            ref = w.at[piece(h, c, 0, 1)]
            return remote(ref, ref, qs.at[rnd, h, c], qr.at[rnd, h, c], z, y, tp)

        def second(h, off, c, s, di, d):
            ref = w.at[place(h, off, s, d)]
            zz, yy = moved(h, 2, d)
            return remote(ref, ref, ss.at[h, di, s, c], rs.at[h, di, s + 1, c], zz, yy, tp)

        def second_in(h, off, c, s, di, d):
            ref = w.at[place(h, off, s, d)]
            return remote(ref, ref, ss.at[h, di, 0, c], rs.at[h, di, s, c], z, y, tp)

        def offset(c):
            return jnp.where(c % 2 == 1, -((c + 1) // 2), c // 2)

        def start(c):
            for h in range(2):
                if c == 0:
                    first(h, 0, 1).start()
                    if n > 2:
                        first(h, 0, 2).start()
                else:
                    first_in(h, c).wait_recv()
                    if c + 2 < n:
                        first(h, c, c + 2).start()
                off = -((c + 1) // 2) if c % 2 else c // 2
                for di, d in ((0, 1), (1, -1)):
                    if half > 1 or di == c % 2:
                        second(h, off, c, 0, di, d).start()

        def pass_on(s, c):
            off = offset(c)
            for h in range(2):
                for di, d in ((0, 1), (1, -1)):
                    second_in(h, off, c, s, di, d).wait_recv()
                if s < half - 1:
                    for di, d in ((0, 1), (1, -1)):
                        second(h, off, c, s, di, d).start()
                else:
                    di = c % 2
                    second(h, off, c, s, di, 1 - 2 * di).start()

        def advance(lo, hi):
            while lo < hi:
                s, c = divmod(lo, n)
                if s == 0:
                    start(c)
                    lo += 1
                elif s < half:
                    stop = min(hi, (s + 1) * n)

                    @pl.loop(c, c + stop - lo)
                    def _(cc, s=s):
                        pass_on(s, cc)

                    lo = stop
                else:
                    stop = min(hi, (s + 1) * n)

                    @pl.loop(c, c + stop - lo)
                    def _(cc, s=s):
                        di = cc % 2
                        for h in range(2):
                            second_in(h, offset(cc), cc, s, di, 1 - 2 * di).wait_recv()

                    lo = stop

        def drain():
            for h in range(2):
                for c in range(1, n):
                    first_in(h, c).wait_send()

            @pl.loop(0, n)
            def _(c):
                off = offset(c)
                for h in range(2):
                    for s in range(half - 1):
                        for di, d in ((0, 1), (1, -1)):
                            second(h, off, c, s, di, d).wait_send()
                    di = c % 2
                    second(h, off, c, half - 1, di, 1 - 2 * di).wait_send()

        return advance, drain

    turns = (half + 1) * n
    ring1, drain1 = ring_one(w1, s1, r1, ps, pr, 0)
    ring2, drain2 = ring_one(w2, s2, r2, ps, pr, 1)

    def block(t):
        return abuf.at[pl.ds(pl.multiple_of(EDGE + rows * t, 16), rows), :]

    def a_out(k):
        return remote(block(tp), block(tp), asem.at[0, k], arem.at[0, k], z, y, ((cx + k) % nx) * 2 + core)

    def a_in(k):
        t = ((cx + nx - k) % nx) * 2 + core
        return remote(block(t), block(t), asem.at[0, k], arem.at[0, k], z, y, tp)

    def a_pair(k):
        t = ((cx + nx - k) % nx) * 2 + core
        return remote(block(t), block(t), asem.at[1, k], arem.at[1, k], z, y, cx * 2 + 1 - core)

    def a_pair_in(k):
        t = ((cx + nx - k) % nx) * 2 + 1 - core
        return remote(block(t), block(t), asem.at[1, k], arem.at[1, k], z, y, tp)

    before = abuf.at[pl.ds(0, EDGE), :]
    after = abuf.at[pl.ds(EDGE + length, EDGE), :]
    last_own = abuf.at[pl.ds(EDGE + length - EDGE, EDGE), :]
    first_own = abuf.at[pl.ds(EDGE, EDGE), :]
    down = (sp + n * n - 1) % (n * n)
    up = (sp + 1) % (n * n)
    far = tps - 1

    def edge_next():
        return remote(last_own, before, hs.at[0, 0], hr.at[0, 0], up // n, up % n, far)

    def edge_prev():
        return remote(first_own, after, hs.at[1, 0], hr.at[1, 0], down // n, down % n, 0)

    def edge_share(side, k):
        ref = (before, after)[side]
        return remote(ref, ref, hs.at[side, k], hr.at[side, k], z, y, ((far, 0)[side] + k) % tps)

    def edge_share_in(side, k):
        ref = (before, after)[side]
        return remote(ref, ref, hs.at[side, k], hr.at[side, k], z, y, tp)

    @pl.when((tp == far) & (sp < n * n - 1))
    def _():
        edge_next().start()

    @pl.when((tp == 0) & (sp > 0))
    def _():
        edge_prev().start()

    for k in range(1, nx):
        a_out(k).start()
    a_pair(0).start()

    ring1(0, n)

    @pl.when((tp == far) & (sp > 0))
    def _():
        edge_share_in(0, 0).wait_recv()
        for k in range(1, tps):
            edge_share(0, k).start()

    @pl.when((tp == 0) & (sp < n * n - 1))
    def _():
        edge_share_in(1, 0).wait_recv()
        for k in range(1, tps):
            edge_share(1, k).start()

    ring1(n, min(2 * n, half * n))
    for k in range(1, nx):
        if k != half_way(nx):
            a_in(k).wait_recv()
            a_pair(k).start()
    ring1(min(2 * n, half * n), half * n)
    if nx > 1:
        a_in(half_way(nx)).wait_recv()
        a_pair(half_way(nx)).start()
    ring2(0, 1)
    ring1(half * n, turns)
    for k in range(nx):
        a_pair_in(k).wait_recv()

    for side in range(2):
        edge_there = (sp > 0) if side == 0 else (sp < n * n - 1)
        for k in range(1, tps):

            @pl.when(edge_there & (tp == ((far, 0)[side] + k) % tps))
            def _(side=side, k=k):
                edge_share_in(side, k).wait_recv()

    tall = length + 2 * EDGE

    def project1(lo, hi):
        got = jnp.dot(abuf[...], w1[:, :, :, :, lo:hi].reshape(dim, hi - lo), preferred_element_type=F32)
        p1[:, lo:hi] = wide(got.astype(BF))

    tb = 128 if length % 128 == 0 else rows

    def mix(lo):
        if lo == 0:
            taps = wide(xtap_ref[...])
        else:
            at = lo - 128
            taps = wide(ltap_ref[:, at // 256, at % 256 : at % 256 + 128])
        for b in range(length // tb):
            acc = None
            for k in range(5):
                term = p1[EDGE - 2 + k + b * tb : EDGE - 2 + k + (b + 1) * tb, lo : lo + 128] * taps[k : k + 1, :]
                acc = term if acc is None else acc + term
            mixed[b * tb : (b + 1) * tb, lo : lo + 128] = silu(acc).astype(BF)

    project1(0, 256)
    ring2(1, 3)
    project1(256, 512)
    project1(512, 640)
    ring2(3, min(5, n))
    for j in range(5):
        mix(128 * j)

    steps = jnp.concatenate([step_ref[0], step_ref[1], jnp.zeros((12, dim), BF)], axis=0)
    raw = dot_nt(steps, abuf[EDGE : EDGE + length, :])[0:8]
    deltas = softplus(wide(raw.astype(BF)))
    spike = spike_ref[...]
    spikes = jnp.concatenate([spike, spike, jnp.zeros((4, length), F32)], axis=0)
    row_id = lax.broadcasted_iota(jnp.int32, (8, 1), 0)
    rates = jnp.zeros((8, 1), F32)
    for k in range(4):
        rates = jnp.where(row_id == k, rate_ref[k // 2, k % 2], rates)
    logs = spikes - deltas * rates
    logs = jnp.where(row_id < 4, logs, 0.0)
    lane = lax.broadcasted_iota(jnp.int32, (8, length), 1)
    fsum = logs
    bsum = logs
    shift = 1
    while shift < length:
        fsum = fsum + jnp.where(lane >= shift, pltpu.roll(fsum, shift, axis=1), 0.0)
        bsum = bsum + jnp.where(lane < length - shift, pltpu.roll(bsum, length - shift, axis=1), 0.0)
        shift *= 2
    run = jnp.where(row_id < 2, fsum, bsum)
    total = jnp.where(row_id < 2, fsum[:, length - 1 : length], bsum[:, 0:1])
    weight = jnp.exp(total - run) * deltas
    turned = jnp.concatenate([run, weight, jnp.exp(run), jnp.zeros((CH - 24, length), F32)], axis=0).T

    low = lax.broadcasted_iota(jnp.int32, (length, CH), 1) < HEAD
    xs_all = wide(mixed[:, 0:128])
    states = []
    for d in range(2):
        w_d = jnp.where(low, turned[:, 8 + 2 * d : 9 + 2 * d], turned[:, 9 + 2 * d : 10 + 2 * d])
        xw = (xs_all * w_d).astype(BF)
        for h in range(2):
            full = dot_tn(xw, mixed[:, 128 + 128 * h : 256 + 128 * h])
            states.append(full[HEAD * h : HEAD * h + HEAD, :])
    decay = jnp.broadcast_to(jnp.exp(total), (8, STATE))

    def packed(parts, dec):
        high = dec.astype(BF)
        rest = dec - wide(high)
        return jnp.concatenate([*parts, wide(high), rest], axis=0).astype(BF)

    for j in range(n):
        got = packed([s[sl * j : sl * j + sl, :] for s in states], decay)
        sb1[j] = got
    rb1[y] = sb1[y]

    def e1(k):
        yy = (y + k) % n
        return remote(sb1.at[yy], rb1.at[y], es.at[0, k], er.at[0, k], z, yy, tp)

    def e2(k):
        return remote(sb2, rb2.at[z], es.at[1, k], er.at[1, k], (z + k) % n, y, tp)

    def e3(k):
        yy = (y + k) % n
        return remote(sb3.at[yy], rb3.at[y], es.at[2, k], er.at[2, k], z, yy, tp)

    def e_in(which, k):
        if which == 0:
            ref = rb1.at[(y - k + n) % n]
        elif which == 1:
            ref = rb2.at[(z - k + n) % n]
        else:
            ref = rb3.at[(y - k + n) % n]
        return remote(ref, ref, es.at[which, k], er.at[which, k], z, y, tp)

    for k in range(1, n):
        e1(k).start()

    runs = [run[k : k + 1, :] for k in range(4)]
    dels = [deltas[k : k + 1, :] for k in range(4)]

    def within(h, b):
        scores = dot_nt(
            mixed[b * tb : (b + 1) * tb, 384 + 128 * h : 512 + 128 * h],
            mixed[:, 128 + 128 * h : 256 + 128 * h],
        )
        t_id = lax.broadcasted_iota(jnp.int32, (tb, length), 0) + b * tb
        s_id = lax.broadcasted_iota(jnp.int32, (tb, length), 1)
        part = turned[b * tb : (b + 1) * tb, :]
        gap_f = part[:, h : h + 1] - runs[h]
        gap_b = part[:, 2 + h : 3 + h] - runs[2 + h]
        factor = jnp.where(s_id < t_id, dels[h], jnp.where(s_id > t_id, dels[2 + h], dels[h] + dels[2 + h]))
        decays = jnp.exp(jnp.where(s_id < t_id, gap_f, jnp.where(s_id > t_id, gap_b, 0.0)))
        weights = (scores * decays * factor).astype(BF)
        keep = (lax.broadcasted_iota(jnp.int32, (length, CH), 1) // HEAD) == h
        x_h = jnp.where(keep, xs_all, 0.0).astype(BF)
        got = jnp.dot(weights, x_h, preferred_element_type=F32)
        at = slice(b * tb, (b + 1) * tb)
        yacc[at, :] = got if h == 0 else yacc[at, :] + got

    spots = [(h, b) for h in range(2) for b in range(length // tb)]
    at_turn = min(5, n)
    for i, (h, b) in enumerate(spots):
        within(h, b)
        to = min(n, at_turn + 1)
        ring2(at_turn, to)
        at_turn = to

    for k in range(1, n):
        e_in(0, k).wait_recv()

    def opened(ref):
        blk = wide(ref[...])
        parts = [blk[sl * q : sl * q + sl, :] for q in range(4)]
        base = 4 * sl
        decs = [blk[base + q : base + q + 1, :] + blk[base + 8 + q : base + 9 + q, :] for q in range(4)]
        return parts, decs

    carry = [jnp.zeros((sl, STATE), F32) for _ in range(4)]
    prod = [jnp.ones((1, STATE), F32) for _ in range(4)]
    for j in range(n):
        for q in range(4):
            jj = j if q < 2 else n - 1 - j
            blk = wide(rb1[jj])
            pre[jj, sl * q : sl * q + sl, :] = carry[q]
            prd[jj, q : q + 1, :] = prod[q]
            dec = blk[4 * sl + q : 4 * sl + q + 1, :] + blk[4 * sl + 8 + q : 4 * sl + 9 + q, :]
            carry[q] = carry[q] * dec + blk[sl * q : sl * q + sl, :]
            prod[q] = prod[q] * dec
    prods = jnp.concatenate([*prod, jnp.zeros((4, STATE), F32)], axis=0)
    sb2[...] = packed(carry, prods)
    for k in range(1, n):
        e2(k).start()
    to = min(2 * n, half * n)
    ring2(at_turn, max(at_turn, to))
    at_turn = max(at_turn, to)
    for k in range(1, n):
        e_in(1, k).wait_recv()
    entry = [jnp.zeros((sl, STATE), F32) for _ in range(4)]
    for j in range(n):
        for q in range(4):
            jj = j if q < 2 else n - 1 - j
            blk = wide(rb2[jj])
            dec = blk[4 * sl + q : 4 * sl + q + 1, :] + blk[4 * sl + 8 + q : 4 * sl + 9 + q, :]
            ahead = (jj < z) if q < 2 else (jj > z)
            entry[q] = jnp.where(ahead, entry[q] * dec + blk[sl * q : sl * q + sl, :], entry[q])
    for j in range(n):
        parts = [entry[q] * prd[j, q : q + 1, :] + pre[j, sl * q : sl * q + sl, :] for q in range(4)]
        sb3[j] = jnp.concatenate(parts, axis=0).astype(BF)
    rb3[y] = sb3[y]
    for k in range(1, n):
        e3(k).start()

    ring2(at_turn, half * n)
    ring2(half * n, turns)

    def project2(lo, hi):
        got = jnp.dot(abuf[...], w2[:, :, :, :, lo:hi].reshape(dim, hi - lo), preferred_element_type=F32)
        p2[:, lo:hi] = wide(got.astype(BF))

    project2(0, 256)
    project2(256, 512)
    p2[:, 128:256] = wide((p2[:, 128:256] * p2[:, 256:384]).astype(BF))
    ctaps = wide(ctap_ref[...])
    for b in range(length // tb):
        acc = None
        for k in range(3):
            term = p2[EDGE - 1 + k + b * tb : EDGE - 1 + k + (b + 1) * tb, 128:256] * ctaps[k : k + 1, :]
            acc = term if acc is None else acc + term
        ycat[b * tb : (b + 1) * tb, 0:128] = (p2[EDGE + b * tb : EDGE + (b + 1) * tb, 0:128] * acc).astype(BF)

    for k in range(1, n):
        e_in(2, k).wait_recv()
    blocks = [wide(rb3[j]) for j in range(n)]
    arrived = [
        jnp.concatenate([blk[sl * q : sl * q + sl, :] for blk in blocks], axis=0).astype(BF) for q in range(4)
    ]
    none = jnp.zeros((HEAD, STATE), BF)
    y_all = yacc[...]
    for d in range(2):
        top = jnp.concatenate([arrived[2 * d], none], axis=1)
        bottom = jnp.concatenate([none, arrived[2 * d + 1]], axis=1)
        into = dot_nt(mixed[:, 384:640], jnp.concatenate([top, bottom], axis=0))
        grow = jnp.where(low, turned[:, 16 + 2 * d : 17 + 2 * d], turned[:, 17 + 2 * d : 18 + 2 * d])
        y_all = y_all + into * grow
    g = y_all * silu(p2[EDGE : EDGE + length, 384:512])
    sq = g * g
    mean0 = jnp.sum(jnp.where(low, sq, 0.0), axis=-1, keepdims=True) / HEAD
    mean1 = jnp.sum(jnp.where(low, 0.0, sq), axis=-1, keepdims=True) / HEAD
    inv = jnp.where(low, lax.rsqrt(mean0 + EPS), lax.rsqrt(mean1 + EPS))
    ycat[:, 128:256] = (g * inv * wide(lane_ref[...])).astype(BF)

    def to_pair(c):
        cols = slice(c * wcol, (c + 1) * wcol)
        return remote(
            obf.at[:, 1 - core, :, cols], prx.at[:, :, cols], os_.at[c], or_.at[c], z, y, cx * 2 + 1 - core
        )

    def to_owner(c, k):
        cols = slice(c * wcol, (c + 1) * wcol)
        xx = (cx + k) % nx
        return remote(
            xsend.at[xx, :, cols], xrecv.at[k, :, cols], xs.at[c, k], xr.at[c, k], z, y, xx * 2 + core
        )

    exits = w2[:, :, :, :, 512:768].reshape(dim, 2 * CH)
    for c in range(ncol):
        cols = slice(c * wcol, (c + 1) * wcol)
        got = dot_nt(ycat[...], exits[c * wcol : (c + 1) * wcol, :])
        obf[:, :, :, cols] = got.astype(BF).reshape(nx, 2, rows, wcol)
        to_pair(c).start()
    for c in range(ncol):
        cols = slice(c * wcol, (c + 1) * wcol)
        to_pair(c).wait_recv()
        for xx in range(nx):
            both = wide(obf[xx, core, :, cols]) + wide(prx[xx, :, cols])
            xsend[xx, :, cols] = both.astype(BF)
        for k in range(1, nx):
            to_owner(c, k).start()
    drain1()
    drain2()
    for c in range(ncol):
        cols = slice(c * wcol, (c + 1) * wcol)
        both = wide(obf[cx, core, :, cols]) + wide(prx[cx, :, cols])
        for k in range(1, nx):
            to_owner(c, k).wait_recv()
            both = both + wide(xrecv[k, :, cols])
        out_ref[:, cols] = both.astype(BF)

    for c in range(ncol):
        to_pair(c).wait_send()
        for k in range(1, nx):
            to_owner(c, k).wait_send()
    for k in range(1, n):
        e1(k).wait_send()
        e2(k).wait_send()
        e3(k).wait_send()
    for k in range(1, nx):
        a_out(k).wait_send()
    for k in range(nx):
        a_pair(k).wait_send()

    @pl.when((tp == far) & (sp < n * n - 1))
    def _():
        edge_next().wait_send()

    @pl.when((tp == 0) & (sp > 0))
    def _():
        edge_prev().wait_send()

    @pl.when((tp == far) & (sp > 0))
    def _():
        for k in range(1, tps):
            edge_share(0, k).wait_send()

    @pl.when((tp == 0) & (sp < n * n - 1))
    def _():
        for k in range(1, tps):
            edge_share(1, k).wait_send()


def half_way(nx):
    return nx // 2


def run_layer(n, tps, ncol, *args):
    (
        x,
        gain,
        slide,
        rec,
        lat,
        step,
        ctap,
        xtap,
        ltap,
        rate,
        spike,
        lane,
        cexit,
        sexit,
    ) = args
    rows, dim = x.shape
    length = rows * tps
    tall = length + 2 * EDGE
    nx = tps // 2
    half = n // 2
    sl = HEAD // n
    vm = pltpu.VMEM
    dma = pltpu.SemaphoreType.DMA
    vmem = pl.BlockSpec(memory_space=pltpu.VMEM)
    specs = [vmem] * 14
    specs[9] = pl.BlockSpec(memory_space=pltpu.SMEM)
    return pl.pallas_call(
        functools.partial(layer, n, tps),
        out_shape=jax.ShapeDtypeStruct((rows, dim), BF),
        in_specs=specs,
        out_specs=vmem,
        scratch_shapes=[
            vm((tall, dim), BF),
            vm((n, n, 2, 16, 640), BF),
            vm((n, n, 2, 16, 768), BF),
            vm((tall, 640), F32),
            vm((tall, 512), F32),
            vm((length, 640), BF),
            vm((length, 256), BF),
            vm((length, 128), F32),
            vm((n, 4 * sl + 16, STATE), BF),
            vm((n, 4 * sl + 16, STATE), BF),
            vm((4 * sl + 16, STATE), BF),
            vm((n, 4 * sl + 16, STATE), BF),
            vm((n, 4 * sl, STATE), BF),
            vm((n, 4 * sl, STATE), BF),
            vm((n, 4 * sl, STATE), F32),
            vm((n, 8, STATE), F32),
            vm((nx, 2, rows, dim), BF),
            vm((nx, rows, dim), BF),
            vm((nx, rows, dim), BF),
            vm((nx, rows, dim), BF),
            dma((2, 2, half + 1, n)),
            dma((2, 2, half + 1, n)),
            dma((2, 2, half + 1, n)),
            dma((2, 2, half + 1, n)),
            dma((2, 2, n)),
            dma((2, 2, n)),
            dma((2, nx)),
            dma((2, nx)),
            dma((2, tps)),
            dma((2, tps)),
            dma((3, n)),
            dma((3, n)),
            dma((ncol,)),
            dma((ncol,)),
            dma((ncol, nx)),
            dma((ncol, nx)),
        ],
        compiler_params=pltpu.CompilerParams(
            collective_id=0, has_side_effects=True, vmem_limit_bytes=60 * 1024 * 1024
        ),
        name="layer",
    )(
        x,
        gain.reshape(1, dim),
        slide,
        rec,
        lat,
        step.transpose(1, 2, 0),
        ctap,
        xtap,
        ltap,
        rate,
        spike.T,
        lane.reshape(1, CH),
        cexit.T,
        sexit.T,
    )


def solution(mesh):
    n = 8 if mesh.shape["sp"] == 64 else int(round(mesh.shape["sp"] ** 0.5))
    sp_tp = ("sp", "tp")
    return jax.shard_map(
        functools.partial(run_layer, n, mesh.shape["tp"], 4),
        mesh=mesh,
        in_specs=(
            P(sp_tp, None),
            P(),
            P(None, "sp", "tp"),
            P(None, "sp", "tp"),
            P(None, "sp", "tp"),
            P(None, None, "tp"),
            P(None, "tp"),
            P(None, "tp"),
            P(None, None, "tp"),
            P(None, "tp"),
            P("sp", "tp"),
            P("tp"),
            P("tp", "sp"),
            P("tp", "sp"),
        ),
        out_specs=P(sp_tp, None),
        check_vma=False,
    )
```

time: 294 us -> 98.8 us (0.34)
  blocking collectives: 161 us -> 0 us
  Pallas kernels: 0 us -> 95.6 us
  waiting for transfers between devices: 41 us -> 0 us
  local copies, waits for them, and re-layouts: 31.4 us -> 2.91 us
  other arithmetic: 15.3 us -> 0 us
  between operations: 15.3 us -> 0.01 us
  starting transfers between devices: 14.7 us -> 0 us
  matrix products: 13.9 us -> 0 us
    all_gather x5 -> x0, blocking collectives: 97.1 us -> none  [the longest x3 55.6 us: carried_in(): lax.all_gather(part.astype(kind), axis)]
    pallas_call x0 -> x1, Pallas kernels: none -> 95.6 us  [run_layer(): pl.pallas_call(functools.partial(layer, n, tps), out_shape=jax.ShapeDtype...]
    all_to_all x1 -> x0, blocking collectives: 52.2 us -> none  [sum_at_owner(): lax.all_to_all(cut_along(value, dim, length), axis, 0, 0, tiled=True)]
    all_gather x1 -> x0, waiting for transfers between devices: 19.5 us -> none  [gather_turned(): out = lax.all_gather(both, axis, axis=0, tiled=True)]
    all_to_all x1 -> x0, waiting for transfers between devices: 18 us -> none  [from_everyone(): lax.all_to_all(jnp.broadcast_to(value[None], (length, *value.shape)), axi...]
    dot_general x12 -> x0, matrix products: 13.9 us -> none  [the longest x1 2.41 us: local(): jnp.einsum('rd,kdc->rkc', row_piece, sliding_mixer_entry_matrix, preferre...]
    unnamed x1 -> x0, blocking collectives: 11.3 us -> none
    all_to_all x1 -> x0, starting transfers between devices: 10.5 us -> none  [from_everyone(): lax.all_to_all(jnp.broadcast_to(value[None], (length, *value.shape)), axi...]
  transfers between devices with their start and end apart: 4 -> 0, of which waited for: 3 -> 0; matrix products, arithmetic and copies ran while one was open for 5% -> 0% of each run, Pallas kernels for 0% -> 0%
where the time goes in v1:
time: 98.8 us; the launch traced here: 98.6 us
  Pallas kernels  95.6 us (97%)
  local copies, waits for them, and re-layouts  2.91 us (3%)
    pallas_call x1, Pallas kernels, run_layer(): pl.pallas_call(functools.partial(layer, n, tps), out_shape=jax.ShapeDtype...  95.6 us
    unnamed x3, local copies, waits for them, and re-layouts  2.3 us

profile of v1, /device:TPU:1, one launch (start us, length us, event | category | flops | bytes accessed | tf_op | source)
XLA Modules:
  0.0 98.6 jit_solution(10345394890681824495)
XLA Ops:
  0.0 0.0 copy-start
  0.0 0.7 copy-done
  0.7 0.6 reshape.6.gain_ref
  1.3 95.6 %layer.1 = bf16[48,2048]{1,0:T(8,128)(2,1)} custom-call(bf16[48,2048]{1,0:T(8,128)(2,1)} %x_ref.1, bf16[1,2048]{1,0:T(2,128)(2,1)} %reshape.6.gain_ref, bf16[3,32,128]{2,1,0:T(8,128)(2,1)} %slide_ref.1, bf16[2,32,128]{2,1,0:T(8,128)(2,1)} %rec_ref.1, bf16[2,32,256]{2,1,0:T(8,128)(2,1)} %lat_ref.1, bf16[2,2,2048]{2,1,0:T(2,128)(2,1)} %bitcast.5, ...), custom_call_target="tpu_custom_call" | custom-call | tf_op jit(solution)/shard_map/layer/pallas_call | solution.py:669
  96.9 1.6 %copy.16 = bf16[48,2048]{1,0:T(8,128)(2,1)} copy(bf16[48,2048]{1,0:T(8,128)(2,1)} %layer.1) | data formatting | bytes 393216
Async XLA Ops:
  0.0 0.7 copy-start

commit v2 on v1

--- a/solution.py
+++ b/solution.py
@@ -40,20 +40,20 @@
 def layer(
     n,
     tps,
-    x_ref,
-    gain_ref,
-    slide_ref,
-    rec_ref,
-    lat_ref,
-    step_ref,
-    ctap_ref,
-    xtap_ref,
-    ltap_ref,
-    rate_ref,
-    spike_ref,
-    lane_ref,
-    cexit_ref,
-    sexit_ref,
+    x_hbm,
+    gain_hbm,
+    slide_hbm,
+    rec_hbm,
+    lat_hbm,
+    step_hbm,
+    ctap_hbm,
+    xtap_hbm,
+    ltap_hbm,
+    rate_hbm,
+    spike_hbm,
+    lane_hbm,
+    cexit_hbm,
+    sexit_hbm,
     out_ref,
     abuf,
     w1,
@@ -91,6 +91,21 @@
     or_,
     xs,
     xr,
+    x_ref,
+    gain_ref,
+    slide_ref,
+    rec_ref,
+    lat_ref,
+    step_ref,
+    ctap_ref,
+    xtap_ref,
+    ltap_ref,
+    rate_ref,
+    spike_ref,
+    lane_ref,
+    cexit_ref,
+    sexit_ref,
+    ins,
 ):
     rows = x_ref.shape[0]
     dim = x_ref.shape[1]
@@ -117,6 +132,26 @@
             device_id_type=MESH_IDS,
         )
 
+    given = (
+        (x_hbm, x_ref),
+        (gain_hbm, gain_ref),
+        (slide_hbm, slide_ref),
+        (rec_hbm, rec_ref),
+        (lat_hbm, lat_ref),
+        (step_hbm, step_ref),
+        (ctap_hbm, ctap_ref),
+        (xtap_hbm, xtap_ref),
+        (ltap_hbm, ltap_ref),
+        (rate_hbm, rate_ref),
+        (spike_hbm, spike_ref),
+        (lane_hbm, lane_ref),
+        (cexit_hbm, cexit_ref),
+        (sexit_hbm, sexit_ref),
+    )
+    loads = [pltpu.make_async_copy(src, dst, ins.at[i]) for i, (src, dst) in enumerate(given)]
+    for load in loads:
+        load.start()
+
     bar = pltpu.get_barrier_semaphore()
 
     def greet(s, t):
@@ -130,10 +165,15 @@
     greet((sp + 1) % (n * n), tp)
     greet((sp + n * n - 1) % (n * n), tp)
 
+    for load in loads:
+        load.wait()
     xf = wide(x_ref[...])
     scale = lax.rsqrt(jnp.mean(xf * xf, axis=-1, keepdims=True) + EPS)
     own_rows = pl.ds(pl.multiple_of(EDGE + rows * tp, 16), rows)
-    abuf[own_rows, :] = (xf * scale * wide(gain_ref[...])).astype(BF)
+    gains = wide(gain_ref[...])
+    for j in range(dim // 128):
+        cols = slice(128 * j, 128 * j + 128)
+        abuf[own_rows, cols] = (xf[:, cols] * scale * gains[j : j + 1, :]).astype(BF)
 
     @pl.when(sp == 0)
     def _():
@@ -170,7 +210,7 @@
             return (z - d * s + n) % n, (y + off + n) % n, 0
         return (z + off + n) % n, (y - d * s + n) % n, 1
 
-    def ring_one(w, ss, rs, qs, qr, rnd):
+    def ring_one(w, ss, rs, qs, qr, rnd, straight):
         def first(h, c, nxt):
             d = 1 if nxt % 2 else -1
             ref = w.at[piece(h, c, 0, 1)]
@@ -193,16 +233,33 @@
         def offset(c):
             return jnp.where(c % 2 == 1, -((c + 1) // 2), c // 2)
 
+        def direct(h, c):
+            d = (c + 1) // 2 if c % 2 else -(c // 2)
+            ref = w.at[piece(h, 0, 0, 1)]
+            zz, yy = moved(h, 1, d)
+            return remote(ref, ref, qs.at[rnd, h, c], qr.at[rnd, h, c], zz, yy, tp)
+
+        def spread(lo, hi):
+            for c in range(lo, hi):
+                for h in range(2):
+                    direct(h, c).start()
+
+        def lead(lo, hi):
+            for c in range(lo, hi):
+                for h in range(2):
+                    if c == 0:
+                        first(h, 0, 1).start()
+                        if n > 2:
+                            first(h, 0, 2).start()
+                    else:
+                        first_in(h, c).wait_recv()
+                        if c + 2 < n:
+                            first(h, c, c + 2).start()
+
         def start(c):
             for h in range(2):
-                if c == 0:
-                    first(h, 0, 1).start()
-                    if n > 2:
-                        first(h, 0, 2).start()
-                else:
+                if straight and c > 0:
                     first_in(h, c).wait_recv()
-                    if c + 2 < n:
-                        first(h, c, c + 2).start()
                 off = -((c + 1) // 2) if c % 2 else c // 2
                 for di, d in ((0, 1), (1, -1)):
                     if half > 1 or di == c % 2:
@@ -260,11 +317,11 @@
                     di = c % 2
                     second(h, off, c, half - 1, di, 1 - 2 * di).wait_send()
 
-        return advance, drain
+        return advance, drain, spread, lead
 
     turns = (half + 1) * n
-    ring1, drain1 = ring_one(w1, s1, r1, ps, pr, 0)
-    ring2, drain2 = ring_one(w2, s2, r2, ps, pr, 1)
+    ring1, drain1, spread1, _ = ring_one(w1, s1, r1, ps, pr, 0, True)
+    ring2, drain2, _, lead2 = ring_one(w2, s2, r2, ps, pr, 1, False)
 
     def block(t):
         return abuf.at[pl.ds(pl.multiple_of(EDGE + rows * t, 16), rows), :]
@@ -306,19 +363,27 @@
         ref = (before, after)[side]
         return remote(ref, ref, hs.at[side, k], hr.at[side, k], z, y, tp)
 
-    @pl.when((tp == far) & (sp < n * n - 1))
-    def _():
-        edge_next().start()
-
-    @pl.when((tp == 0) & (sp > 0))
-    def _():
-        edge_prev().start()
-
+    spread1(1, 3)
+    ring1(0, 1)
+    spread1(3, n)
     for k in range(1, nx):
         a_out(k).start()
     a_pair(0).start()
 
-    ring1(0, n)
+    @pl.when((tp == far) & (sp < n * n - 1))
+    def _():
+        edge_next().start()
+
+    @pl.when((tp == 0) & (sp > 0))
+    def _():
+        edge_prev().start()
+
+    ring1(1, 3)
+    lead2(0, 1)
+    ring1(n, n + 1)
+    ring1(3, 5)
+    ring1(n + 1, n + 3)
+    ring1(5, n)
 
     @pl.when((tp == far) & (sp > 0))
     def _():
@@ -332,17 +397,21 @@
         for k in range(1, tps):
             edge_share(1, k).start()
 
-    ring1(n, min(2 * n, half * n))
+    lead2(1, 3)
+    ring1(n + 3, 2 * n)
     for k in range(1, nx):
         if k != half_way(nx):
             a_in(k).wait_recv()
             a_pair(k).start()
-    ring1(min(2 * n, half * n), half * n)
-    if nx > 1:
-        a_in(half_way(nx)).wait_recv()
-        a_pair(half_way(nx)).start()
-    ring2(0, 1)
-    ring1(half * n, turns)
+    lead2(3, 5)
+    ring1(2 * n, 3 * n)
+    a_in(half_way(nx)).wait_recv()
+    a_pair(half_way(nx)).start()
+    lead2(5, 7)
+    ring1(3 * n, 4 * n)
+    lead2(7, 8)
+    ring2(0, 4)
+
     for k in range(nx):
         a_pair_in(k).wait_recv()
 
@@ -353,35 +422,6 @@
             @pl.when(edge_there & (tp == ((far, 0)[side] + k) % tps))
             def _(side=side, k=k):
                 edge_share_in(side, k).wait_recv()
-
-    tall = length + 2 * EDGE
-
-    def project1(lo, hi):
-        got = jnp.dot(abuf[...], w1[:, :, :, :, lo:hi].reshape(dim, hi - lo), preferred_element_type=F32)
-        p1[:, lo:hi] = wide(got.astype(BF))
-
-    tb = 128 if length % 128 == 0 else rows
-
-    def mix(lo):
-        if lo == 0:
-            taps = wide(xtap_ref[...])
-        else:
-            at = lo - 128
-            taps = wide(ltap_ref[:, at // 256, at % 256 : at % 256 + 128])
-        for b in range(length // tb):
-            acc = None
-            for k in range(5):
-                term = p1[EDGE - 2 + k + b * tb : EDGE - 2 + k + (b + 1) * tb, lo : lo + 128] * taps[k : k + 1, :]
-                acc = term if acc is None else acc + term
-            mixed[b * tb : (b + 1) * tb, lo : lo + 128] = silu(acc).astype(BF)
-
-    project1(0, 256)
-    ring2(1, 3)
-    project1(256, 512)
-    project1(512, 640)
-    ring2(3, min(5, n))
-    for j in range(5):
-        mix(128 * j)
 
     steps = jnp.concatenate([step_ref[0], step_ref[1], jnp.zeros((12, dim), BF)], axis=0)
     raw = dot_nt(steps, abuf[EDGE : EDGE + length, :])[0:8]
@@ -391,7 +431,7 @@
     row_id = lax.broadcasted_iota(jnp.int32, (8, 1), 0)
     rates = jnp.zeros((8, 1), F32)
     for k in range(4):
-        rates = jnp.where(row_id == k, rate_ref[k // 2, k % 2], rates)
+        rates = jnp.where(row_id == k, rate_ref[k // 2 : k // 2 + 1, k % 2 : k % 2 + 1], rates)
     logs = spikes - deltas * rates
     logs = jnp.where(row_id < 4, logs, 0.0)
     lane = lax.broadcasted_iota(jnp.int32, (8, length), 1)
@@ -406,6 +446,42 @@
     total = jnp.where(row_id < 2, fsum[:, length - 1 : length], bsum[:, 0:1])
     weight = jnp.exp(total - run) * deltas
     turned = jnp.concatenate([run, weight, jnp.exp(run), jnp.zeros((CH - 24, length), F32)], axis=0).T
+
+    ring1(4 * n, turns)
+    ring2(4, 6)
+
+    def project1(lo, hi):
+        w = w1[:, :, :, :, lo:hi].reshape(dim, hi - lo)
+        if hi - lo > 128:
+            got = jnp.dot(abuf[...], w, preferred_element_type=F32)
+        else:
+            cut = dim // 2
+            got = jnp.dot(abuf[:, :cut], w[:cut], preferred_element_type=F32)
+            got = got + jnp.dot(abuf[:, cut:], w[cut:], preferred_element_type=F32)
+        p1[:, lo:hi] = wide(got.astype(BF))
+
+    tb = 128 if length % 128 == 0 else rows
+
+    def mix(lo):
+        if lo == 0:
+            taps = wide(xtap_ref[...])
+        else:
+            at = lo - 128
+            taps = wide(ltap_ref[:, at // 256, at % 256 : at % 256 + 128])
+        for b in range(length // tb):
+            acc = None
+            for k in range(5):
+                term = p1[EDGE - 2 + k + b * tb : EDGE - 2 + k + (b + 1) * tb, lo : lo + 128] * taps[k : k + 1, :]
+                acc = term if acc is None else acc + term
+            mixed[b * tb : (b + 1) * tb, lo : lo + 128] = silu(acc).astype(BF)
+
+    project1(0, 512)
+    ring2(6, 9)
+    project1(512, 640)
+    ring2(9, 11)
+    for j in range(5):
+        mix(128 * j)
+    ring2(11, 12)
 
     low = lax.broadcasted_iota(jnp.int32, (length, CH), 1) < HEAD
     xs_all = wide(mixed[:, 0:128])
@@ -474,12 +550,10 @@
         yacc[at, :] = got if h == 0 else yacc[at, :] + got
 
     spots = [(h, b) for h in range(2) for b in range(length // tb)]
-    at_turn = min(5, n)
+    ring2(12, 13)
     for i, (h, b) in enumerate(spots):
         within(h, b)
-        to = min(n, at_turn + 1)
-        ring2(at_turn, to)
-        at_turn = to
+        ring2(13 + i, 14 + i)
 
     for k in range(1, n):
         e_in(0, k).wait_recv()
@@ -506,9 +580,7 @@
     sb2[...] = packed(carry, prods)
     for k in range(1, n):
         e2(k).start()
-    to = min(2 * n, half * n)
-    ring2(at_turn, max(at_turn, to))
-    at_turn = max(at_turn, to)
+    ring2(19, 24)
     for k in range(1, n):
         e_in(1, k).wait_recv()
     entry = [jnp.zeros((sl, STATE), F32) for _ in range(4)]
@@ -526,8 +598,7 @@
     for k in range(1, n):
         e3(k).start()
 
-    ring2(at_turn, half * n)
-    ring2(half * n, turns)
+    ring2(24, turns)
 
     def project2(lo, hi):
         got = jnp.dot(abuf[...], w2[:, :, :, :, lo:hi].reshape(dim, hi - lo), preferred_element_type=F32)
@@ -664,8 +735,23 @@
     vm = pltpu.VMEM
     dma = pltpu.SemaphoreType.DMA
     vmem = pl.BlockSpec(memory_space=pltpu.VMEM)
-    specs = [vmem] * 14
-    specs[9] = pl.BlockSpec(memory_space=pltpu.SMEM)
+    specs = [pl.BlockSpec(memory_space=pltpu.HBM)] * 14
+    operands = (
+        x,
+        gain.reshape(dim // 128, 128),
+        slide,
+        rec,
+        lat,
+        step.transpose(1, 2, 0),
+        ctap,
+        xtap,
+        ltap,
+        rate,
+        spike.T,
+        lane.reshape(1, CH),
+        cexit.T,
+        sexit.T,
+    )
     return pl.pallas_call(
         functools.partial(layer, n, tps),
         out_shape=jax.ShapeDtypeStruct((rows, dim), BF),
@@ -708,27 +794,14 @@
             dma((ncol,)),
             dma((ncol, nx)),
             dma((ncol, nx)),
+            *[vm(v.shape, v.dtype) for v in operands],
+            dma((14,)),
         ],
         compiler_params=pltpu.CompilerParams(
             collective_id=0, has_side_effects=True, vmem_limit_bytes=60 * 1024 * 1024
         ),
         name="layer",
-    )(
-        x,
-        gain.reshape(1, dim),
-        slide,
-        rec,
-        lat,
-        step.transpose(1, 2, 0),
-        ctap,
-        xtap,
-        ltap,
-        rate,
-        spike.T,
-        lane.reshape(1, CH),
-        cexit.T,
-        sexit.T,
-    )
+    )(*operands)
 
 
 def solution(mesh):

time: 98.8 us -> 84 us (0.85)
  Pallas kernels: 95.6 us -> 82.3 us
  local copies, waits for them, and re-layouts: 2.91 us -> 1.62 us
    pallas_call x1, Pallas kernels: 95.6 us -> 82.3 us  [run_layer(): pl.pallas_call(functools.partial(layer, n, tps), out_shape=jax.ShapeDtype...]
    unnamed x3 -> x1, local copies, waits for them, and re-layouts: 2.3 us -> 1.62 us
where the time goes in v2:
time: 84 us; the launch traced here: 83.9 us
  Pallas kernels  82.3 us (98%)
  local copies, waits for them, and re-layouts  1.62 us (2%)
    pallas_call x1, Pallas kernels, run_layer(): pl.pallas_call(functools.partial(layer, n, tps), out_shape=jax.ShapeDtype...  82.3 us

profile of v2, /device:TPU:1, one launch (start us, length us, event | category | flops | bytes accessed | tf_op | source)
XLA Modules:
  0.0 83.9 jit_solution(4059196050053456694)
XLA Ops:
  0.0 82.3 %layer.1 = bf16[48,2048]{1,0:T(8,128)(2,1)} custom-call(bf16[48,2048]{1,0:T(8,128)(2,1)} %x_hbm.1, bf16[16,128]{1,0:T(8,128)(2,1)} %bitcast.9, bf16[3,32,128]{2,1,0:T(8,128)(2,1)} %slide_hbm.1, bf16[2,32,128]{2,1,0:T(8,128)(2,1)} %rec_hbm.1, bf16[2,32,256]{2,1,0:T(8,128)(2,1)} %lat_hbm.1, bf16[2,2,2048]{2,1,0:T(2,128)(2,1)} %bitcast.6, ...), custom_call_target="tpu_custom_call" | custom-call | tf_op jit(solution)/shard_map/layer/pallas_call | solution.py:755
  82.3 1.6 %copy.16 = bf16[48,2048]{1,0:T(8,128)(2,1)} copy(bf16[48,2048]{1,0:T(8,128)(2,1)} %layer.1) | data formatting | bytes 393216

commit v3 on v2

--- a/solution.py
+++ b/solution.py
@@ -75,6 +75,7 @@
     prx,
     xsend,
     xrecv,
+    lrecv,
     s1,
     r1,
     s2,
@@ -113,7 +114,7 @@
     length = rows * tps
     half = n // 2
     sl = HEAD // n
-    ncol = os_.shape[0]
+    ncol = or_.shape[0]
     wcol = dim // ncol
     sp = lax.axis_index("sp")
     tp = lax.axis_index("tp")
@@ -215,20 +216,20 @@
             d = 1 if nxt % 2 else -1
             ref = w.at[piece(h, c, 0, 1)]
             zz, yy = moved(h, 1, d)
-            return remote(ref, ref, qs.at[rnd, h, nxt], qr.at[rnd, h, nxt], zz, yy, tp)
-
-        def first_in(h, c):
-            ref = w.at[piece(h, c, 0, 1)]
-            return remote(ref, ref, qs.at[rnd, h, c], qr.at[rnd, h, c], z, y, tp)
+            return remote(ref, ref, qs.at[rnd], qr.at[rnd, nxt], zz, yy, tp)
+
+        def first_in(c):
+            ref = w.at[0, 0]
+            remote(ref, ref, qs.at[rnd], qr.at[rnd, c], z, y, tp).wait_recv()
 
         def second(h, off, c, s, di, d):
             ref = w.at[place(h, off, s, d)]
             zz, yy = moved(h, 2, d)
-            return remote(ref, ref, ss.at[h, di, s, c], rs.at[h, di, s + 1, c], zz, yy, tp)
-
-        def second_in(h, off, c, s, di, d):
-            ref = w.at[place(h, off, s, d)]
-            return remote(ref, ref, ss.at[h, di, 0, c], rs.at[h, di, s, c], z, y, tp)
+            return remote(ref, ref, ss.at[0], rs.at[s, c], zz, yy, tp)
+
+        def second_in(c, s):
+            ref = w.at[0, 0:2] if s < half else w.at[0, 0]
+            remote(ref, ref, ss.at[0], rs.at[s - 1, c], z, y, tp).wait_recv()
 
         def offset(c):
             return jnp.where(c % 2 == 1, -((c + 1) // 2), c // 2)
@@ -237,7 +238,7 @@
             d = (c + 1) // 2 if c % 2 else -(c // 2)
             ref = w.at[piece(h, 0, 0, 1)]
             zz, yy = moved(h, 1, d)
-            return remote(ref, ref, qs.at[rnd, h, c], qr.at[rnd, h, c], zz, yy, tp)
+            return remote(ref, ref, qs.at[rnd], qr.at[rnd, c], zz, yy, tp)
 
         def spread(lo, hi):
             for c in range(lo, hi):
@@ -246,20 +247,19 @@
 
         def lead(lo, hi):
             for c in range(lo, hi):
+                if c > 0:
+                    first_in(c)
                 for h in range(2):
                     if c == 0:
                         first(h, 0, 1).start()
-                        if n > 2:
-                            first(h, 0, 2).start()
-                    else:
-                        first_in(h, c).wait_recv()
-                        if c + 2 < n:
-                            first(h, c, c + 2).start()
+                        first(h, 0, 2).start()
+                    elif c + 2 < n:
+                        first(h, c, c + 2).start()
 
         def start(c):
+            if straight and c > 0:
+                first_in(c)
             for h in range(2):
-                if straight and c > 0:
-                    first_in(h, c).wait_recv()
                 off = -((c + 1) // 2) if c % 2 else c // 2
                 for di, d in ((0, 1), (1, -1)):
                     if half > 1 or di == c % 2:
@@ -267,9 +267,8 @@
 
         def pass_on(s, c):
             off = offset(c)
+            second_in(c, s)
             for h in range(2):
-                for di, d in ((0, 1), (1, -1)):
-                    second_in(h, off, c, s, di, d).wait_recv()
                 if s < half - 1:
                     for di, d in ((0, 1), (1, -1)):
                         second(h, off, c, s, di, d).start()
@@ -296,26 +295,15 @@
 
                     @pl.loop(c, c + stop - lo)
                     def _(cc, s=s):
-                        di = cc % 2
-                        for h in range(2):
-                            second_in(h, offset(cc), cc, s, di, 1 - 2 * di).wait_recv()
+                        second_in(cc, s)
 
                     lo = stop
 
         def drain():
-            for h in range(2):
-                for c in range(1, n):
-                    first_in(h, c).wait_send()
-
-            @pl.loop(0, n)
-            def _(c):
-                off = offset(c)
-                for h in range(2):
-                    for s in range(half - 1):
-                        for di, d in ((0, 1), (1, -1)):
-                            second(h, off, c, s, di, d).wait_send()
-                    di = c % 2
-                    second(h, off, c, half - 1, di, 1 - 2 * di).wait_send()
+            lead_all = w.at[0, 0 : n - 1]
+            remote(lead_all, lead_all, qs.at[rnd], qr.at[rnd, 0], z, y, tp).wait_send()
+            ring_all = w.at[0 : n - 1]
+            remote(ring_all, ring_all, ss.at[0], rs.at[0, 0], z, y, tp).wait_send()
 
         return advance, drain, spread, lead
 
@@ -327,19 +315,19 @@
         return abuf.at[pl.ds(pl.multiple_of(EDGE + rows * t, 16), rows), :]
 
     def a_out(k):
-        return remote(block(tp), block(tp), asem.at[0, k], arem.at[0, k], z, y, ((cx + k) % nx) * 2 + core)
+        return remote(block(tp), block(tp), asem.at[0], arem.at[k], z, y, ((cx + k) % nx) * 2 + core)
 
     def a_in(k):
         t = ((cx + nx - k) % nx) * 2 + core
-        return remote(block(t), block(t), asem.at[0, k], arem.at[0, k], z, y, tp)
+        return remote(block(t), block(t), asem.at[0], arem.at[k], z, y, tp)
 
     def a_pair(k):
         t = ((cx + nx - k) % nx) * 2 + core
-        return remote(block(t), block(t), asem.at[1, k], arem.at[1, k], z, y, cx * 2 + 1 - core)
-
-    def a_pair_in(k):
-        t = ((cx + nx - k) % nx) * 2 + 1 - core
-        return remote(block(t), block(t), asem.at[1, k], arem.at[1, k], z, y, tp)
+        return remote(block(t), block(t), asem.at[1], arem.at[nx], z, y, cx * 2 + 1 - core)
+
+    def a_wait(blocks, which):
+        ref = abuf.at[pl.ds(0, rows * blocks), :]
+        return remote(ref, ref, asem.at[which], arem.at[nx], z, y, tp)
 
     before = abuf.at[pl.ds(0, EDGE), :]
     after = abuf.at[pl.ds(EDGE + length, EDGE), :]
@@ -350,18 +338,22 @@
     far = tps - 1
 
     def edge_next():
-        return remote(last_own, before, hs.at[0, 0], hr.at[0, 0], up // n, up % n, far)
+        return remote(last_own, before, hs.at[0, 0], hr.at[0], up // n, up % n, far)
 
     def edge_prev():
-        return remote(first_own, after, hs.at[1, 0], hr.at[1, 0], down // n, down % n, 0)
+        return remote(first_own, after, hs.at[1, 0], hr.at[1], down // n, down % n, 0)
 
     def edge_share(side, k):
         ref = (before, after)[side]
-        return remote(ref, ref, hs.at[side, k], hr.at[side, k], z, y, ((far, 0)[side] + k) % tps)
-
-    def edge_share_in(side, k):
+        return remote(ref, ref, hs.at[side, 1], hr.at[side], z, y, ((far, 0)[side] + k) % tps)
+
+    def edge_in(side):
         ref = (before, after)[side]
-        return remote(ref, ref, hs.at[side, k], hr.at[side, k], z, y, tp)
+        remote(ref, ref, hs.at[side, 1], hr.at[side], z, y, tp).wait_recv()
+
+    def edge_sent(side):
+        ref = abuf.at[pl.ds(0, EDGE * (tps - 1)), :]
+        remote(ref, ref, hs.at[side, 1], hr.at[side], z, y, tp).wait_send()
 
     spread1(1, 3)
     ring1(0, 1)
@@ -387,13 +379,13 @@
 
     @pl.when((tp == far) & (sp > 0))
     def _():
-        edge_share_in(0, 0).wait_recv()
+        edge_in(0)
         for k in range(1, tps):
             edge_share(0, k).start()
 
     @pl.when((tp == 0) & (sp < n * n - 1))
     def _():
-        edge_share_in(1, 0).wait_recv()
+        edge_in(1)
         for k in range(1, tps):
             edge_share(1, k).start()
 
@@ -412,16 +404,15 @@
     lead2(7, 8)
     ring2(0, 4)
 
-    for k in range(nx):
-        a_pair_in(k).wait_recv()
-
-    for side in range(2):
-        edge_there = (sp > 0) if side == 0 else (sp < n * n - 1)
-        for k in range(1, tps):
-
-            @pl.when(edge_there & (tp == ((far, 0)[side] + k) % tps))
-            def _(side=side, k=k):
-                edge_share_in(side, k).wait_recv()
+    a_wait(nx, 1).wait_recv()
+
+    @pl.when((tp != far) & (sp > 0))
+    def _():
+        edge_in(0)
+
+    @pl.when((tp != 0) & (sp < n * n - 1))
+    def _():
+        edge_in(1)
 
     steps = jnp.concatenate([step_ref[0], step_ref[1], jnp.zeros((12, dim), BF)], axis=0)
     raw = dot_nt(steps, abuf[EDGE : EDGE + length, :])[0:8]
@@ -506,23 +497,18 @@
 
     def e1(k):
         yy = (y + k) % n
-        return remote(sb1.at[yy], rb1.at[y], es.at[0, k], er.at[0, k], z, yy, tp)
+        return remote(sb1.at[yy], rb1.at[y], es.at[0], er.at[0], z, yy, tp)
 
     def e2(k):
-        return remote(sb2, rb2.at[z], es.at[1, k], er.at[1, k], (z + k) % n, y, tp)
+        return remote(sb2, rb2.at[z], es.at[1], er.at[1], (z + k) % n, y, tp)
 
     def e3(k):
         yy = (y + k) % n
-        return remote(sb3.at[yy], rb3.at[y], es.at[2, k], er.at[2, k], z, yy, tp)
-
-    def e_in(which, k):
-        if which == 0:
-            ref = rb1.at[(y - k + n) % n]
-        elif which == 1:
-            ref = rb2.at[(z - k + n) % n]
-        else:
-            ref = rb3.at[(y - k + n) % n]
-        return remote(ref, ref, es.at[which, k], er.at[which, k], z, y, tp)
+        return remote(sb3.at[yy], rb3.at[y], es.at[2], er.at[2], z, yy, tp)
+
+    def e_all(which):
+        ref = (rb1, rb2, rb3)[which].at[0 : n - 1]
+        return remote(ref, ref, es.at[which], er.at[which], z, y, tp)
 
     for k in range(1, n):
         e1(k).start()
@@ -555,8 +541,7 @@
         within(h, b)
         ring2(13 + i, 14 + i)
 
-    for k in range(1, n):
-        e_in(0, k).wait_recv()
+    e_all(0).wait_recv()
 
     def opened(ref):
         blk = wide(ref[...])
@@ -581,8 +566,7 @@
     for k in range(1, n):
         e2(k).start()
     ring2(19, 24)
-    for k in range(1, n):
-        e_in(1, k).wait_recv()
+    e_all(1).wait_recv()
     entry = [jnp.zeros((sl, STATE), F32) for _ in range(4)]
     for j in range(n):
         for q in range(4):
@@ -615,8 +599,7 @@
             acc = term if acc is None else acc + term
         ycat[b * tb : (b + 1) * tb, 0:128] = (p2[EDGE + b * tb : EDGE + (b + 1) * tb, 0:128] * acc).astype(BF)
 
-    for k in range(1, n):
-        e_in(2, k).wait_recv()
+    e_all(2).wait_recv()
     blocks = [wide(rb3[j]) for j in range(n)]
     arrived = [
         jnp.concatenate([blk[sl * q : sl * q + sl, :] for blk in blocks], axis=0).astype(BF) for q in range(4)
@@ -636,55 +619,73 @@
     inv = jnp.where(low, lax.rsqrt(mean0 + EPS), lax.rsqrt(mean1 + EPS))
     ycat[:, 128:256] = (g * inv * wide(lane_ref[...])).astype(BF)
 
+    def span(c):
+        return slice(c * wcol, (c + 1) * wcol)
+
     def to_pair(c):
-        cols = slice(c * wcol, (c + 1) * wcol)
         return remote(
-            obf.at[:, 1 - core, :, cols], prx.at[:, :, cols], os_.at[c], or_.at[c], z, y, cx * 2 + 1 - core
+            obf.at[:, 1 - core, :, span(c)], prx.at[:, :, span(c)], os_.at[0], or_.at[c], z, y, cx * 2 + 1 - core
         )
 
-    def to_owner(c, k):
-        cols = slice(c * wcol, (c + 1) * wcol)
-        xx = (cx + k) % nx
+    right = (cx + 1) % nx
+    left = (cx + nx - 1) % nx
+    opposite = (cx + 2) % nx
+
+    def relay(c):
+        xx = right if c < ncol // 2 else left
         return remote(
-            xsend.at[xx, :, cols], xrecv.at[k, :, cols], xs.at[c, k], xr.at[c, k], z, y, xx * 2 + core
+            xsend.at[opposite, :, span(c)], lrecv.at[:, span(c)], xs.at[0], xr.at[0, c], z, y, xx * 2 + core
         )
 
+    def to_owner(c, side):
+        xx = (right, left)[side]
+        return remote(
+            xsend.at[xx, :, span(c)], xrecv.at[side, :, span(c)], xs.at[1], xr.at[1, c], z, y, xx * 2 + core
+        )
+
+    def owner_in(c):
+        ref = xrecv.at[:, :, span(c)]
+        remote(ref, ref, xs.at[1], xr.at[1, c], z, y, tp).wait_recv()
+
+    def chip_sum(xx, c):
+        return wide(obf[xx, core, :, span(c)]) + wide(prx[xx, :, span(c)])
+
+    order = [c for pair in zip(range(ncol // 2), range(ncol // 2, ncol)) for c in pair]
     exits = w2[:, :, :, :, 512:768].reshape(dim, 2 * CH)
-    for c in range(ncol):
-        cols = slice(c * wcol, (c + 1) * wcol)
+    for c in order:
         got = dot_nt(ycat[...], exits[c * wcol : (c + 1) * wcol, :])
-        obf[:, :, :, cols] = got.astype(BF).reshape(nx, 2, rows, wcol)
+        obf[:, :, :, span(c)] = got.astype(BF).reshape(nx, 2, rows, wcol)
         to_pair(c).start()
-    for c in range(ncol):
-        cols = slice(c * wcol, (c + 1) * wcol)
+    for c in order:
         to_pair(c).wait_recv()
-        for xx in range(nx):
-            both = wide(obf[xx, core, :, cols]) + wide(prx[xx, :, cols])
-            xsend[xx, :, cols] = both.astype(BF)
-        for k in range(1, nx):
-            to_owner(c, k).start()
+        xsend[opposite, :, span(c)] = chip_sum(opposite, c).astype(BF)
+        relay(c).start()
+        side = 1 if c < ncol // 2 else 0
+        xx = (right, left)[side]
+        xsend[xx, :, span(c)] = chip_sum(xx, c).astype(BF)
+        to_owner(c, side).start()
+    for c in order:
+        relay(c).wait_recv()
+        side = 0 if c < ncol // 2 else 1
+        xx = (right, left)[side]
+        xsend[xx, :, span(c)] = (chip_sum(xx, c) + wide(lrecv[:, span(c)])).astype(BF)
+        to_owner(c, side).start()
     drain1()
     drain2()
-    for c in range(ncol):
-        cols = slice(c * wcol, (c + 1) * wcol)
-        both = wide(obf[cx, core, :, cols]) + wide(prx[cx, :, cols])
-        for k in range(1, nx):
-            to_owner(c, k).wait_recv()
-            both = both + wide(xrecv[k, :, cols])
-        out_ref[:, cols] = both.astype(BF)
-
-    for c in range(ncol):
-        to_pair(c).wait_send()
-        for k in range(1, nx):
-            to_owner(c, k).wait_send()
-    for k in range(1, n):
-        e1(k).wait_send()
-        e2(k).wait_send()
-        e3(k).wait_send()
-    for k in range(1, nx):
-        a_out(k).wait_send()
-    for k in range(nx):
-        a_pair(k).wait_send()
+    for c in order:
+        own = chip_sum(cx, c)
+        owner_in(c)
+        out_ref[:, span(c)] = (own + wide(xrecv[0, :, span(c)]) + wide(xrecv[1, :, span(c)])).astype(BF)
+
+    remote(prx, prx, os_.at[0], or_.at[0], z, y, tp).wait_send()
+    relayed = xsend.at[0]
+    remote(relayed, relayed, xs.at[0], xr.at[0, 0], z, y, tp).wait_send()
+    owned = xsend.at[0:2]
+    remote(owned, owned, xs.at[1], xr.at[1, 0], z, y, tp).wait_send()
+    for which in range(3):
+        e_all(which).wait_send()
+    a_wait(nx - 1, 0).wait_send()
+    a_wait(nx, 1).wait_send()
 
     @pl.when((tp == far) & (sp < n * n - 1))
     def _():
@@ -696,13 +697,11 @@
 
     @pl.when((tp == far) & (sp > 0))
     def _():
-        for k in range(1, tps):
-            edge_share(0, k).wait_send()
+        edge_sent(0)
 
     @pl.when((tp == 0) & (sp < n * n - 1))
     def _():
-        for k in range(1, tps):
-            edge_share(1, k).wait_send()
+        edge_sent(1)
 
 
 def half_way(nx):
@@ -777,23 +776,24 @@
             vm((nx, 2, rows, dim), BF),
             vm((nx, rows, dim), BF),
             vm((nx, rows, dim), BF),
-            vm((nx, rows, dim), BF),
-            dma((2, 2, half + 1, n)),
-            dma((2, 2, half + 1, n)),
-            dma((2, 2, half + 1, n)),
-            dma((2, 2, half + 1, n)),
-            dma((2, 2, n)),
-            dma((2, 2, n)),
-            dma((2, nx)),
-            dma((2, nx)),
-            dma((2, tps)),
-            dma((2, tps)),
-            dma((3, n)),
-            dma((3, n)),
+            vm((2, rows, dim), BF),
+            vm((rows, dim), BF),
+            dma((1,)),
+            dma((half, n)),
+            dma((1,)),
+            dma((half, n)),
+            dma((2,)),
+            dma((2, n)),
+            dma((2,)),
+            dma((1 + nx,)),
+            dma((2, 2)),
+            dma((2,)),
+            dma((3,)),
+            dma((3,)),
+            dma((1,)),
             dma((ncol,)),
-            dma((ncol,)),
-            dma((ncol, nx)),
-            dma((ncol, nx)),
+            dma((2,)),
+            dma((2, ncol)),
             *[vm(v.shape, v.dtype) for v in operands],
             dma((14,)),
         ],

time: 84 us -> 75 us (0.89)
  Pallas kernels: 82.3 us -> 73.2 us
    pallas_call x1, Pallas kernels: 82.3 us -> 73.2 us  [run_layer(): pl.pallas_call(functools.partial(layer, n, tps), out_shape=jax.ShapeDtype...]
where the time goes in v3:
time: 75 us; the launch traced here: 74.8 us
  Pallas kernels  73.2 us (98%)
  local copies, waits for them, and re-layouts  1.62 us (2%)
    pallas_call x1, Pallas kernels, run_layer(): pl.pallas_call(functools.partial(layer, n, tps), out_shape=jax.ShapeDtype...  73.2 us
    unnamed x1, local copies, waits for them, and re-layouts  1.62 us

profile of v3, /device:TPU:1, one launch (start us, length us, event | category | flops | bytes accessed | tf_op | source)
XLA Modules:
  0.0 74.8 jit_solution(17841327194094359315)
XLA Ops:
  0.0 73.2 %layer.1 = bf16[48,2048]{1,0:T(8,128)(2,1)} custom-call(bf16[48,2048]{1,0:T(8,128)(2,1)} %x_hbm.1, bf16[16,128]{1,0:T(8,128)(2,1)} %bitcast.9, bf16[3,32,128]{2,1,0:T(8,128)(2,1)} %slide_hbm.1, bf16[2,32,128]{2,1,0:T(8,128)(2,1)} %rec_hbm.1, bf16[2,32,256]{2,1,0:T(8,128)(2,1)} %lat_hbm.1, bf16[2,2,2048]{2,1,0:T(2,128)(2,1)} %bitcast.6, ...), custom_call_target="tpu_custom_call" | custom-call | tf_op jit(solution)/shard_map/layer/pallas_call | solution.py:754
  73.2 1.6 %copy.16 = bf16[48,2048]{1,0:T(8,128)(2,1)} copy(bf16[48,2048]{1,0:T(8,128)(2,1)} %layer.1) | data formatting | bytes 393216

commit v4 on v3

--- a/solution.py
+++ b/solution.py
@@ -446,9 +446,10 @@
         if hi - lo > 128:
             got = jnp.dot(abuf[...], w, preferred_element_type=F32)
         else:
-            cut = dim // 2
-            got = jnp.dot(abuf[:, :cut], w[:cut], preferred_element_type=F32)
-            got = got + jnp.dot(abuf[:, cut:], w[cut:], preferred_element_type=F32)
+            cut = (length + 2 * EDGE) // 2
+            top = jnp.dot(abuf[:cut, :], w, preferred_element_type=F32)
+            low_part = jnp.dot(abuf[cut:, :], w, preferred_element_type=F32)
+            got = jnp.concatenate([top, low_part], axis=0)
         p1[:, lo:hi] = wide(got.astype(BF))
 
     tb = 128 if length % 128 == 0 else rows
@@ -488,7 +489,7 @@
     def packed(parts, dec):
         high = dec.astype(BF)
         rest = dec - wide(high)
-        return jnp.concatenate([*parts, wide(high), rest], axis=0).astype(BF)
+        return jnp.concatenate([*parts, wide(high)[0:4], rest[0:4]], axis=0).astype(BF)
 
     for j in range(n):
         got = packed([s[sl * j : sl * j + sl, :] for s in states], decay)
@@ -541,14 +542,8 @@
         within(h, b)
         ring2(13 + i, 14 + i)
 
+    ring2(19, 22)
     e_all(0).wait_recv()
-
-    def opened(ref):
-        blk = wide(ref[...])
-        parts = [blk[sl * q : sl * q + sl, :] for q in range(4)]
-        base = 4 * sl
-        decs = [blk[base + q : base + q + 1, :] + blk[base + 8 + q : base + 9 + q, :] for q in range(4)]
-        return parts, decs
 
     carry = [jnp.zeros((sl, STATE), F32) for _ in range(4)]
     prod = [jnp.ones((1, STATE), F32) for _ in range(4)]
@@ -558,21 +553,21 @@
             blk = wide(rb1[jj])
             pre[jj, sl * q : sl * q + sl, :] = carry[q]
             prd[jj, q : q + 1, :] = prod[q]
-            dec = blk[4 * sl + q : 4 * sl + q + 1, :] + blk[4 * sl + 8 + q : 4 * sl + 9 + q, :]
+            dec = blk[4 * sl + q : 4 * sl + q + 1, :] + blk[4 * sl + 4 + q : 4 * sl + 5 + q, :]
             carry[q] = carry[q] * dec + blk[sl * q : sl * q + sl, :]
             prod[q] = prod[q] * dec
     prods = jnp.concatenate([*prod, jnp.zeros((4, STATE), F32)], axis=0)
     sb2[...] = packed(carry, prods)
     for k in range(1, n):
         e2(k).start()
-    ring2(19, 24)
+    ring2(22, 29)
     e_all(1).wait_recv()
     entry = [jnp.zeros((sl, STATE), F32) for _ in range(4)]
     for j in range(n):
         for q in range(4):
             jj = j if q < 2 else n - 1 - j
             blk = wide(rb2[jj])
-            dec = blk[4 * sl + q : 4 * sl + q + 1, :] + blk[4 * sl + 8 + q : 4 * sl + 9 + q, :]
+            dec = blk[4 * sl + q : 4 * sl + q + 1, :] + blk[4 * sl + 4 + q : 4 * sl + 5 + q, :]
             ahead = (jj < z) if q < 2 else (jj > z)
             entry[q] = jnp.where(ahead, entry[q] * dec + blk[sl * q : sl * q + sl, :], entry[q])
     for j in range(n):
@@ -582,7 +577,7 @@
     for k in range(1, n):
         e3(k).start()
 
-    ring2(24, turns)
+    ring2(29, turns)
 
     def project2(lo, hi):
         got = jnp.dot(abuf[...], w2[:, :, :, :, lo:hi].reshape(dim, hi - lo), preferred_element_type=F32)
@@ -753,7 +748,7 @@
     )
     return pl.pallas_call(
         functools.partial(layer, n, tps),
-        out_shape=jax.ShapeDtypeStruct((rows, dim), BF),
+        out_shape=pltpu.VMEM((rows, dim), BF),
         in_specs=specs,
         out_specs=vmem,
         scratch_shapes=[
@@ -765,10 +760,10 @@
             vm((length, 640), BF),
             vm((length, 256), BF),
             vm((length, 128), F32),
-            vm((n, 4 * sl + 16, STATE), BF),
-            vm((n, 4 * sl + 16, STATE), BF),
-            vm((4 * sl + 16, STATE), BF),
-            vm((n, 4 * sl + 16, STATE), BF),
+            vm((n, 4 * sl + 8, STATE), BF),
+            vm((n, 4 * sl + 8, STATE), BF),
+            vm((4 * sl + 8, STATE), BF),
+            vm((n, 4 * sl + 8, STATE), BF),
             vm((n, 4 * sl, STATE), BF),
             vm((n, 4 * sl, STATE), BF),
             vm((n, 4 * sl, STATE), F32),

time: 75 us -> 72.4 us (0.965)
  Pallas kernels: 73.2 us -> 71.6 us
  local copies, waits for them, and re-layouts: 1.62 us -> 0.68 us
    pallas_call x1, Pallas kernels: 73.2 us -> 71.6 us  [run_layer(): pl.pallas_call(functools.partial(layer, n, tps), out_shape=pltpu.VMEM((ro...]
    unnamed x1, local copies, waits for them, and re-layouts: 1.62 us -> 0.68 us
where the time goes in v4:
time: 72.4 us; the launch traced here: 72.2 us
  Pallas kernels  71.6 us (99%)
    pallas_call x1, Pallas kernels, run_layer(): pl.pallas_call(functools.partial(layer, n, tps), out_shape=pltpu.VMEM((ro...  71.6 us

profile of v4, /device:TPU:1, one launch (start us, length us, event | category | flops | bytes accessed | tf_op | source)
XLA Modules:
  0.0 72.2 jit_solution(10034013997130359213)
XLA Ops:
  0.0 71.6 %layer.1 = bf16[48,2048]{1,0:T(8,128)(2,1)S(1)} custom-call(bf16[48,2048]{1,0:T(8,128)(2,1)} %x_hbm.1, bf16[16,128]{1,0:T(8,128)(2,1)} %bitcast.9, bf16[3,32,128]{2,1,0:T(8,128)(2,1)} %slide_hbm.1, bf16[2,32,128]{2,1,0:T(8,128)(2,1)} %rec_hbm.1, bf16[2,32,256]{2,1,0:T(8,128)(2,1)} %lat_hbm.1, bf16[2,2,2048]{2,1,0:T(2,128)(2,1)} %bitcast.6, ...), custom_call_target="tpu_custom_call" | custom-call | tf_op jit(solution)/shard_map/layer/pallas_call | solution.py:749
  71.6 0.7 copy.16

commit v5 on v4

--- a/solution.py
+++ b/solution.py
@@ -560,7 +560,7 @@
     sb2[...] = packed(carry, prods)
     for k in range(1, n):
         e2(k).start()
-    ring2(22, 29)
+    ring2(22, 32)
     e_all(1).wait_recv()
     entry = [jnp.zeros((sl, STATE), F32) for _ in range(4)]
     for j in range(n):
@@ -577,7 +577,7 @@
     for k in range(1, n):
         e3(k).start()
 
-    ring2(29, turns)
+    ring2(32, turns)
 
     def project2(lo, hi):
         got = jnp.dot(abuf[...], w2[:, :, :, :, lo:hi].reshape(dim, hi - lo), preferred_element_type=F32)

time: 72.4 us -> 72.1 us (level)
  no operation moved by 1% of the time
where the time goes in v5:
time: 72.1 us; the launch traced here: 71.9 us
  Pallas kernels  71.3 us (99%)
    pallas_call x1, Pallas kernels, run_layer(): pl.pallas_call(functools.partial(layer, n, tps), out_shape=pltpu.VMEM((ro...  71.3 us

profile of v5, /device:TPU:1, one launch (start us, length us, event | category | flops | bytes accessed | tf_op | source)
XLA Modules:
  0.0 71.9 jit_solution(4225370351614419271)
XLA Ops:
  0.0 71.3 %layer.1 = bf16[48,2048]{1,0:T(8,128)(2,1)S(1)} custom-call(bf16[48,2048]{1,0:T(8,128)(2,1)} %x_hbm.1, bf16[16,128]{1,0:T(8,128)(2,1)} %bitcast.9, bf16[3,32,128]{2,1,0:T(8,128)(2,1)} %slide_hbm.1, bf16[2,32,128]{2,1,0:T(8,128)(2,1)} %rec_hbm.1, bf16[2,32,256]{2,1,0:T(8,128)(2,1)} %lat_hbm.1, bf16[2,2,2048]{2,1,0:T(2,128)(2,1)} %bitcast.6, ...), custom_call_target="tpu_custom_call" | custom-call | tf_op jit(solution)/shard_map/layer/pallas_call | solution.py:749
  71.3 0.7 copy.16

commit v6 on v5

--- a/solution.py
+++ b/solution.py
@@ -655,6 +655,7 @@
         to_pair(c).wait_recv()
         xsend[opposite, :, span(c)] = chip_sum(opposite, c).astype(BF)
         relay(c).start()
+    for c in order:
         side = 1 if c < ncol // 2 else 0
         xx = (right, left)[side]
         xsend[xx, :, span(c)] = chip_sum(xx, c).astype(BF)

time: 72.1 us -> 72.4 us (level)
  no operation moved by 1% of the time
where the time goes in v6:
time: 72.4 us; the launch traced here: 72.3 us
  Pallas kernels  71.6 us (99%)
    pallas_call x1, Pallas kernels, run_layer(): pl.pallas_call(functools.partial(layer, n, tps), out_shape=pltpu.VMEM((ro...  71.6 us

profile of v6, /device:TPU:1, one launch (start us, length us, event | category | flops | bytes accessed | tf_op | source)
XLA Modules:
  0.0 72.3 jit_solution(3060555566276583020)
XLA Ops:
  0.0 71.6 %layer.1 = bf16[48,2048]{1,0:T(8,128)(2,1)S(1)} custom-call(bf16[48,2048]{1,0:T(8,128)(2,1)} %x_hbm.1, bf16[16,128]{1,0:T(8,128)(2,1)} %bitcast.9, bf16[3,32,128]{2,1,0:T(8,128)(2,1)} %slide_hbm.1, bf16[2,32,128]{2,1,0:T(8,128)(2,1)} %rec_hbm.1, bf16[2,32,256]{2,1,0:T(8,128)(2,1)} %lat_hbm.1, bf16[2,2,2048]{2,1,0:T(2,128)(2,1)} %bitcast.6, ...), custom_call_target="tpu_custom_call" | custom-call | tf_op jit(solution)/shard_map/layer/pallas_call | solution.py:750
  71.6 0.7 copy.16
